TPU v7x, 128 devices: a whole 4x4x4 slice. The times are simulated.
128 devices in a mesh: ep: 64 (over z, y, x), tp: 2 (over core).
Axes of the slice: x: 4, y: 4, z: 4, core: 2. Of those that a mesh axis runs over, the one named last changes fastest.
Arguments:
- tokens: bfloat16 [512, 2048], P('ep'), may hold values from -6 to 6
- mixer_norm_gain: float32 [2048], replicated, may hold values from 0.1 to 1.9
- gate_projection_weight: bfloat16 [2048, 2, 2048], P(None, 'tp', 'ep'), may hold values from -0.125 to 0.125
- value_projection_weight: bfloat16 [2048, 2, 2048], P(None, 'tp', 'ep'), may hold values from -0.125 to 0.125
- input_projection_weight: bfloat16 [2048, 1024], P(None, 'tp'), may hold values from -0.125 to 0.125
- output_projection_weight: bfloat16 [2048, 1024], P(None, 'tp'), may hold values from -0.125 to 0.125
- step_projection_weight: bfloat16 [2048, 64], P(None, 'tp'), may hold values from -0.125 to 0.125
- head_step_bias: float32 [64], P('tp'), may hold values from -1 to 1
- head_decay_rate: float32 [64], P('tp'), may hold values from 0.02 to 3
- extra_log_decay: float32 [512, 64], P('ep', 'tp'), may hold values from -0.7 to 0
- value_taps: float32 [4, 4096], P(None, 'tp'), may hold values from -3 to 3
- input_taps: float32 [4, 1024], P(None, 'tp'), may hold values from -3 to 3
- output_taps: float32 [4, 1024], P(None, 'tp'), may hold values from -3 to 3
- prior_values: bfloat16 [512, 3, 4096], P('ep', None, 'tp'), may hold values from -6 to 6
- prior_input_maps: bfloat16 [512, 3, 1024], P('ep', None, 'tp'), may hold values from -6 to 6
- prior_output_maps: bfloat16 [512, 3, 1024], P('ep', None, 'tp'), may hold values from -6 to 6
- head_skip_gain: float32 [64], P('tp'), may hold values from 0.5 to 1.5
- group_norm_gain: float32 [4096], P('tp'), may hold values from 0.1 to 1.9
- mixer_output_weight: bfloat16 [4096, 2048], P('tp', 'ep'), may hold values from -0.09375 to 0.09375
- recurrent_state: float32 [512, 64, 64, 128], P('ep', 'tp'), may hold values from -6 to 6
- expert_norm_gain: float32 [2048], replicated, may hold values from 0.1 to 1.9
- routes: int32 [512, 6], P('ep'), may hold values from 0 to 63, all different within a row; in each aligned block of 8 rows (0 to 7, 8 to 15, ...) at most 2 rows name the same one
- chosen_expert_weight: float32 [512, 6], P('ep'), may hold values from 0.2 to 1
- routed_gate_weight: bfloat16 [64, 2048, 512], P('ep', None, 'tp'), may hold values from -0.125 to 0.125
- routed_up_weight: bfloat16 [64, 2048, 512], P('ep', None, 'tp'), may hold values from -0.125 to 0.125
- routed_down_weight: bfloat16 [64, 512, 2048], P('ep', 'tp'), may hold values from -0.25 to 0.25
- common_gate_weight: bfloat16 [2048, 512], P(None, 'tp'), may hold values from -0.125 to 0.125
- common_up_weight: bfloat16 [2048, 512], P(None, 'tp'), may hold values from -0.125 to 0.125
- common_down_weight: bfloat16 [512, 2048], P('tp'), may hold values from -0.25 to 0.25
Outputs:
- result: bfloat16 [512, 2048], P('ep')
- state_next: float32 [512, 64, 64, 128], P('ep', 'tp')
- next_value: bfloat16 [512, 3, 4096], P('ep', None, 'tp')
- next_input: bfloat16 [512, 3, 1024], P('ep', None, 'tp')
- next_output: bfloat16 [512, 3, 1024], P('ep', None, 'tp')
Inputs may be any that keep to these rules, and one draw needn't show every extreme that they name: `routes`: the 6 experts of a row differ; among the rows of one device (aligned blocks of 8 rows) no expert is named more than 2 times.
All inputs are finite; a program needn't handle non-finite values.
Results may differ from a plain program's by a relative error of at most 0.015.
Values may be sent and summed in bfloat16 or wider, within the bound.
A program may use at most 128 MiB of HBM per device.

v0:
```python
import jax
import jax.numpy as jnp
from jax import lax
from jax.sharding import PartitionSpec as P

D_INNER = 4096
GROUPS = 8


EPSILON = 1e-06


def sent_to_all(value, axis):
    size = lax.axis_size(axis)
    return lax.all_to_all(
        jnp.broadcast_to(value[None], (size, *value.shape)), axis, 0, 0, tiled=True
    )


def laid_out(pieces, dim):
    pieces = jnp.moveaxis(pieces, 0, dim)
    lengths = pieces.shape
    return pieces.reshape(*lengths[:dim], lengths[dim] * lengths[dim + 1], *lengths[dim + 2 :])


def gather_directly(value, axis, dim):
    pieces = sent_to_all(value, axis)
    return laid_out(pieces, dim)


def over_copies(value, axis):
    return sent_to_all(value, axis).astype(jnp.float32).sum(axis=0)


def rms_scale(values, gain_vec):
    values = values.astype(jnp.float32)
    return (
        values * lax.rsqrt(jnp.mean(values * values, axis=-1, keepdims=True) + EPSILON) * gain_vec
    )


def short_conv(past_rows, fresh_row, weight):
    window = jnp.concatenate([past_rows, fresh_row[:, None, :]], axis=1)
    summed = window[:, 0].astype(jnp.float32) * weight[0]
    for offset in range(1, window.shape[1]):
        summed = summed + window[:, offset].astype(jnp.float32) * weight[offset]
    return (jax.nn.silu(summed), window[:, 1:])


def state_step(
    state_prev, value_conv, input_conv, output_conv, timestep_size, step_decay, head_skip_gain
):
    batch_rows, head_count, head_size, state_size = state_prev.shape
    per_group = head_count // (input_conv.shape[1] // state_size)
    value_heads = value_conv.reshape(batch_rows, head_count, head_size)
    input_heads = jnp.repeat(input_conv.reshape(batch_rows, -1, state_size), per_group, axis=1)
    output_heads = jnp.repeat(output_conv.reshape(batch_rows, -1, state_size), per_group, axis=1)
    state_next = (
        step_decay[:, :, None, None] * state_prev
        + (timestep_size[:, :, None] * value_heads)[:, :, :, None] * input_heads[:, :, None, :]
    )
    mixed_heads = (
        jnp.sum(state_next * output_heads[:, :, None, :], axis=-1)
        + head_skip_gain[None, :, None] * value_heads
    )
    return (state_next, mixed_heads.reshape(batch_rows, -1))


def gated_norm(mixed_flat, gate_rows, group_norm_gain, group_width):
    gated_rows = mixed_flat * jax.nn.silu(gate_rows.astype(jnp.float32))
    grouped = gated_rows.reshape(gated_rows.shape[0], -1, group_width)
    grouped = grouped * lax.rsqrt(jnp.mean(grouped * grouped, axis=-1, keepdims=True) + EPSILON)
    return (grouped.reshape(gated_rows.shape[0], -1) * group_norm_gain).astype(jnp.bfloat16)


def expert_partial(arrived, gate_mat, up_mat, down_mat):
    gate_part = jnp.einsum("slcd,ldf->slcf", arrived, gate_mat, preferred_element_type=jnp.float32)
    up_part = jnp.einsum("slcd,ldf->slcf", arrived, up_mat, preferred_element_type=jnp.float32)
    hidden = (jax.nn.silu(gate_part) * up_part).astype(jnp.bfloat16)
    return jnp.einsum("slcf,lfd->slcd", hidden, down_mat, preferred_element_type=jnp.float32)


def shards(
    tokens,
    mixer_norm_gain,
    gate_projection_weight,
    value_projection_weight,
    input_projection_weight,
    output_projection_weight,
    step_projection_weight,
    head_step_bias,
    head_decay_rate,
    extra_log_decay,
    value_taps,
    input_taps,
    output_taps,
    prior_values,
    prior_input_maps,
    prior_output_maps,
    head_skip_gain,
    group_norm_gain,
    mixer_output_weight,
    recurrent_state,
    expert_norm_gain,
    routes,
    chosen_expert_weight,
    routed_gate_weight,
    routed_up_weight,
    routed_down_weight,
    common_gate_weight,
    common_up_weight,
    common_down_weight,
):
    seq_rows, model_width = tokens.shape
    ep_count = lax.axis_size("ep")
    normed = rms_scale(tokens, mixer_norm_gain).astype(jnp.bfloat16)
    both_pieces = jnp.concatenate(
        [
            gate_projection_weight.reshape(model_width, -1),
            value_projection_weight.reshape(model_width, -1),
        ],
        axis=1,
    )
    piece_width = both_pieces.shape[1] // 2
    projected = jnp.dot(
        gather_directly(normed, "ep", 0), both_pieces, preferred_element_type=jnp.float32
    ).astype(jnp.bfloat16)
    returned = lax.all_to_all(projected, "ep", split_axis=0, concat_axis=1, tiled=True).reshape(
        seq_rows, ep_count, 2, piece_width
    )
    gate_rows = returned[:, :, 0].reshape(seq_rows, -1)
    value_rows = returned[:, :, 1].reshape(seq_rows, -1)
    input_rows = jnp.dot(
        normed, input_projection_weight, preferred_element_type=jnp.float32
    ).astype(jnp.bfloat16)
    output_rows = jnp.dot(
        normed, output_projection_weight, preferred_element_type=jnp.float32
    ).astype(jnp.bfloat16)
    step_raw = jnp.dot(normed, step_projection_weight, preferred_element_type=jnp.float32)
    value_conv, next_value = short_conv(prior_values, value_rows, value_taps)
    input_conv, next_input = short_conv(prior_input_maps, input_rows, input_taps)
    output_conv, next_output = short_conv(prior_output_maps, output_rows, output_taps)
    timestep_size = jax.nn.softplus(step_raw + head_step_bias)
    step_decay = jnp.exp(-timestep_size * head_decay_rate + extra_log_decay)
    state_next, mixed_flat = state_step(
        recurrent_state,
        value_conv,
        input_conv,
        output_conv,
        timestep_size,
        step_decay,
        head_skip_gain,
    )
    mixer_rows = gated_norm(mixed_flat, gate_rows, group_norm_gain, D_INNER // GROUPS)
    partial_mix = jnp.dot(
        gather_directly(mixer_rows, "ep", 0),
        mixer_output_weight,
        preferred_element_type=jnp.float32,
    )
    summed_mix = lax.psum(partial_mix.astype(jnp.bfloat16), "tp")
    mixed_out = lax.all_to_all(summed_mix, "ep", split_axis=0, concat_axis=1, tiled=True)
    stream = (tokens.astype(jnp.float32) + mixed_out.astype(jnp.float32)).astype(jnp.bfloat16)
    ffn_rows = rms_scale(stream, expert_norm_gain).astype(jnp.bfloat16)
    shared_hidden = (
        jax.nn.silu(jnp.dot(ffn_rows, common_gate_weight, preferred_element_type=jnp.float32))
        * jnp.dot(ffn_rows, common_up_weight, preferred_element_type=jnp.float32)
    ).astype(jnp.bfloat16)
    shared_out = lax.psum(
        jnp.dot(shared_hidden, common_down_weight, preferred_element_type=jnp.float32).astype(
            jnp.bfloat16
        ),
        "tp",
    ).astype(jnp.float32)
    exp_local = routed_gate_weight.shape[0]
    expert_total = exp_local * ep_count
    topk_count = routes.shape[1]
    capacity = (seq_rows * topk_count + expert_total - 1) // expert_total + 1
    slot_count = expert_total * capacity
    expert_ids = jnp.arange(expert_total, dtype=jnp.int32)
    flat_routes = routes.reshape(-1)
    onehot = (flat_routes[:, None] == expert_ids[None, :]).astype(jnp.int32)
    slot_ids = jnp.sum((jnp.cumsum(onehot, axis=0) - onehot) * onehot, axis=1)
    positions = flat_routes * capacity + slot_ids
    matches = (jnp.arange(slot_count, dtype=jnp.int32)[:, None] == positions[None, :]).reshape(
        slot_count, seq_rows, topk_count
    )
    dispatch_mat = jnp.sum(matches.astype(jnp.float32), axis=2).astype(jnp.bfloat16)
    combine_mat = jnp.sum(jnp.where(matches, chosen_expert_weight[None], 0.0), axis=2)
    outgoing = jnp.dot(dispatch_mat, ffn_rows, preferred_element_type=jnp.float32).astype(
        jnp.bfloat16
    )
    outgoing = outgoing.reshape(ep_count, exp_local, capacity, model_width)
    partial_out = expert_partial(
        lax.all_to_all(outgoing, "ep", split_axis=0, concat_axis=0, tiled=True),
        routed_gate_weight,
        routed_up_weight,
        routed_down_weight,
    )
    summed_out = over_copies(partial_out.astype(jnp.bfloat16), "tp").astype(jnp.float32)
    returned_out = lax.all_to_all(
        summed_out.astype(jnp.bfloat16), "ep", split_axis=0, concat_axis=0, tiled=True
    )
    routed = lax.dot_general(
        combine_mat,
        returned_out.reshape(slot_count, model_width).astype(jnp.float32),
        (((0,), (0,)), ((), ())),
    )
    result = (stream.astype(jnp.float32) + shared_out + routed).astype(jnp.bfloat16)
    return (result, state_next, next_value, next_input, next_output)


def solution(mesh):
    return jax.shard_map(
        shards,
        mesh=mesh,
        in_specs=(
            P("ep", None),
            P(),
            P(None, "tp", "ep"),
            P(None, "tp", "ep"),
            P(None, "tp"),
            P(None, "tp"),
            P(None, "tp"),
            P("tp"),
            P("tp"),
            P("ep", "tp"),
            P(None, "tp"),
            P(None, "tp"),
            P(None, "tp"),
            P("ep", None, "tp"),
            P("ep", None, "tp"),
            P("ep", None, "tp"),
            P("tp"),
            P("tp"),
            P("tp", "ep"),
            P("ep", "tp", None, None),
            P(),
            P("ep", None),
            P("ep", None),
            P("ep", None, "tp"),
            P("ep", None, "tp"),
            P("ep", "tp", None),
            P(None, "tp"),
            P(None, "tp"),
            P("tp", None),
        ),
        out_specs=(
            P("ep", None),
            P("ep", "tp", None, None),
            P("ep", None, "tp"),
            P("ep", None, "tp"),
            P("ep", None, "tp"),
        ),
        check_vma=False,
    )
```

profile of v0, /device:TPU:1, one launch (start us, length us, event | category | flops | bytes accessed | tf_op | source)
XLA Modules:
  0.0 187.8 jit_solution(11333172729135035962)
XLA Ops:
  0.6 1.0 fusion.34
  1.7 0.8 fusion.36
  2.5 1.6 broadcast_in_dim.22
  4.1 12.3 %all-to-all-start = ((bf16[64,8,2048]{2,1,0:T(8,128)(2,1)}), bf16[64,8,2048]{2,1,0:T(8,128)(2,1)}, u32[]{:S(2)}, u32[]{:S(2)}) async-start(bf16[64,8,2048]{2,1,0:T(8,128)(2,1)} %broadcast_in_dim.22), calls=%async_computation | async-start | bytes 4194304 | tf_op jit(solution)/shard_map/all_to_all | solution.py:15
  17.1 1.0 copy-done.1
  19.4 25.4 %all-to-all-done = bf16[64,8,2048]{2,1,0:T(8,128)(2,1)} async-done(((bf16[64,8,2048]{2,1,0:T(8,128)(2,1)}), bf16[64,8,2048]{2,1,0:T(8,128)(2,1)}, u32[]{:S(2)}, u32[]{:S(2)}) %all-to-all-start) | async-done | bytes 2097184 | tf_op jit(solution)/shard_map/all_to_all | solution.py:15
  44.8 2.3 %fusion.7 = bf16[512,64]{0,1:T(8,128)(2,1)S(1)} fusion(bf16[64,8,2048]{2,1,0:T(8,128)(2,1)} %all-to-all-done, bf16[2048,32]{0,1:T(8,128)(2,1)S(1)} %bitcast.172, bf16[2048,32]{0,1:T(8,128)(2,1)S(1)} %bitcast.173), kind=kOutput, calls=%fused_computation.15 | convolution fusion | flops 134774784 | bytes 2424832 | tf_op jit(solution)/shard_map/dot_general | solution.py:125
  48.1 7.2 %all-to-all-start.1 = ((bf16[64,2,256]{2,1,0:T(2,128)(2,1)}), bf16[64,2,256]{2,1,0:T(2,128)(2,1)S(1)}, u32[]{:S(2)}, u32[]{:S(2)}) async-start(bf16[64,2,256]{2,1,0:T(2,128)(2,1)} %reshape.494), calls=%async_computation.1 | async-start | bytes 131072 | tf_op jit(solution)/shard_map/all_to_all | solution.py:128
  59.7 4.1 %all-to-all-done.1 = bf16[64,2,256]{2,1,0:T(2,128)(2,1)S(1)} async-done(((bf16[64,2,256]{2,1,0:T(2,128)(2,1)}), bf16[64,2,256]{2,1,0:T(2,128)(2,1)S(1)}, u32[]{:S(2)}, u32[]{:S(2)}) %all-to-all-start.1) | async-done | bytes 65568 | tf_op jit(solution)/shard_map/all_to_all | solution.py:128
  66.7 0.9 broadcast_multiply_fusion
  67.7 9.4 %multiply_reduce_fusion = (f32[8,32,64]{2,1,0:T(8,128)S(1)}, f32[8,32,64,128]{3,2,1,0:T(8,128)}) fusion(f32[8,32,128]{2,1,0:T(8,128)S(1)} %get-tuple-element.37, f32[8,32,128]{2,1,0:T(8,128)S(1)} %get-tuple-element.38, f32[8,32,64]{2,1,0:T(8,128)S(1)} %get-tuple-element.15, f32[8,32,64,128]{3,2,1,0:T(8,128)} %param.48, f32[8,32]{1,0:T(8,128)} %get-tuple-element.35), kind=kLoop, calls=%fused_computation | loop fusion | flops 10469376 | bytes 17171456 | tf_op jit(solution)/shard_map/reduce_sum | solution.py:63
  77.9 1.6 broadcast_in_dim.25
  79.4 6.1 %all-to-all-start.2 = ((bf16[64,8,2048]{2,1,0:T(8,128)(2,1)}), bf16[64,8,2048]{2,1,0:T(8,128)(2,1)}, u32[]{:S(2)}, u32[]{:S(2)}) async-start(bf16[64,8,2048]{2,1,0:T(8,128)(2,1)} %broadcast_in_dim.25), calls=%async_computation.2 | async-start | bytes 4194304 | tf_op jit(solution)/shard_map/all_to_all | solution.py:15
  86.2 27.2 %all-to-all-done.2 = bf16[64,8,2048]{2,1,0:T(8,128)(2,1)} async-done(((bf16[64,8,2048]{2,1,0:T(8,128)(2,1)}), bf16[64,8,2048]{2,1,0:T(8,128)(2,1)}, u32[]{:S(2)}, u32[]{:S(2)}) %all-to-all-start.2) | async-done | bytes 2097184 | tf_op jit(solution)/shard_map/all_to_all | solution.py:15
  113.4 2.3 %fusion.11 = bf16[512,32]{0,1:T(8,128)(2,1)S(1)} fusion(bf16[2048,32]{0,1:T(8,128)(2,1)S(1)} %copy-done.9, bf16[64,8,2048]{2,1,0:T(8,128)(2,1)} %all-to-all-done.2), kind=kOutput, calls=%fused_computation.17 | convolution fusion | flops 67125248 | bytes 2260992 | tf_op jit(solution)/shard_map/dot_general | solution.py:155
  115.9 6.5 %psum.14 = bf16[64,8,32]{2,1,0:T(8,128)(2,1)S(1)} all-reduce(bf16[64,8,32]{2,1,0:T(8,128)(2,1)S(1)} %bitcast.169), channel_id=1, replica_groups=mesh['ep'=64,'tp'=2] {'tp'}, use_global_device_ids=true, to_apply=%region_4.5 | all-reduce | flops 16384 | bytes 65536 | tf_op jit(solution)/shard_map/psum | solution.py:160
  123.1 5.3 %all-to-all-start.3 = ((bf16[64,2,128]{2,1,0:T(2,128)(2,1)}), bf16[64,2,128]{2,1,0:T(2,128)(2,1)S(1)}, u32[]{:S(2)}, u32[]{:S(2)}) async-start(bf16[64,2,128]{2,1,0:T(2,128)(2,1)} %reshape.496), calls=%async_computation.3 | async-start | bytes 65536 | tf_op jit(solution)/shard_map/all_to_all | solution.py:161
  128.5 8.2 %all-to-all-done.3 = bf16[64,2,128]{2,1,0:T(2,128)(2,1)S(1)} async-done(((bf16[64,2,128]{2,1,0:T(2,128)(2,1)}), bf16[64,2,128]{2,1,0:T(2,128)(2,1)S(1)}, u32[]{:S(2)}, u32[]{:S(2)}) %all-to-all-start.3) | async-done | bytes 32800 | tf_op jit(solution)/shard_map/all_to_all | solution.py:161
  137.6 1.1 reshape.445
  138.8 4.9 %all-to-all-start.4 = ((bf16[64,1,2,2048]{3,2,1,0:T(2,128)(2,1)}), bf16[64,1,2,2048]{3,2,1,0:T(2,128)(2,1)S(1)}, u32[]{:S(2)}, u32[]{:S(2)}) async-start(bf16[64,1,2,2048]{3,2,1,0:T(2,128)(2,1)} %bitcast.35), calls=%async_computation.4 | async-start | bytes 1048576 | tf_op jit(solution)/shard_map/all_to_all | solution.py:194
  145.3 9.6 %all-to-all-done.4 = bf16[64,1,2,2048]{3,2,1,0:T(2,128)(2,1)S(1)} async-done(((bf16[64,1,2,2048]{3,2,1,0:T(2,128)(2,1)}), bf16[64,1,2,2048]{3,2,1,0:T(2,128)(2,1)S(1)}, u32[]{:S(2)}, u32[]{:S(2)}) %all-to-all-start.4) | async-done | bytes 524320 | tf_op jit(solution)/shard_map/all_to_all | solution.py:194
  154.8 1.6 convolution_bitcast_fusion.1
  156.4 2.3 %convolution_convert_fusion = bf16[64,2,2048]{2,0,1:T(8,128)(2,1)S(1)} fusion(bf16[1,256,2048]{2,1,0:T(8,128)(2,1)} %param.54, bf16[1,2048,256]{2,1,0:T(8,128)(2,1)} %param.53, bf16[64,1,2,2048]{3,2,1,0:T(2,128)(2,1)S(1)} %all-to-all-done.4, f32[64,1,2,256]{3,0,2,1:T(8,128)S(1)} %convolution_bitcast_fusion.1), kind=kOutput, calls=%fused_computation.2 | convolution fusion | flops 268894208 | bytes 3276800 | tf_op jit(solution)/shard_map/slcf,lfd->slcd/dot_general | solution.py:80
  158.9 7.1 %all_to_all.54 = bf16[2,64,1,2,2048]{4,1,3,2,0:T(8,128)(2,1)S(1)} all-to-all(bf16[2,64,1,2,2048]{4,1,3,2,0:T(8,128)(2,1)S(1)} %broadcast_in_dim.28), channel_id=1, replica_groups=mesh['ep'=64,'tp'=2] {'tp'}, dimensions={0} | all-to-all | bytes 2097152 | tf_op jit(solution)/shard_map/all_to_all | solution.py:15
  166.0 1.1 reduce_sum.99
  167.1 2.4 %copy.108 = bf16[64,1,2,2048]{3,2,1,0:T(2,128)(2,1)} copy(bf16[64,1,2,2048]{3,0,2,1:T(8,128)(2,1)} %bitcast.166) | data formatting | bytes 1048576 | tf_op jit(solution)/shard_map/reduce_sum | solution.py:32
  169.5 4.6 %all-to-all-start.6 = ((bf16[64,1,2,2048]{3,2,1,0:T(2,128)(2,1)}), bf16[64,1,2,2048]{3,2,1,0:T(2,128)(2,1)S(1)}, u32[]{:S(2)}, u32[]{:S(2)}) async-start(bf16[64,1,2,2048]{3,2,1,0:T(2,128)(2,1)} %copy.108), calls=%async_computation.6 | async-start | bytes 1048576 | tf_op jit(solution)/shard_map/all_to_all | solution.py:200
  174.1 1.5 fusion.65
  175.7 2.3 %convolution_convert_fusion.2 = bf16[8,2048]{1,0:T(8,128)(2,1)S(1)} fusion(bf16[256,2048]{1,0:T(8,128)(2,1)} %param.57, bf16[2048,256]{1,0:T(8,128)(2,1)} %param.56, f32[8,256]{1,0:T(8,128)S(1)} %fusion.65, bf16[8,2048]{1,0:T(8,128)(2,1)S(1)} %get-tuple-element.12, f32[2048]{0:T(1024)S(1)} %copy-done.17, f32[8]{0:T(128)S(1)} %add_rsqrt_fusion.1), kind=kOutput, calls=%fused_computation.6 | convolution fusion | flops 16871424 | bytes 2179104 | tf_op jit(solution)/shard_map/dot_general | solution.py:169
  178.0 3.7 %psum.15 = bf16[8,2048]{1,0:T(8,128)(2,1)S(1)} all-reduce(bf16[8,2048]{1,0:T(8,128)(2,1)S(1)} %convolution_convert_fusion.2), channel_id=1, replica_groups=mesh['ep'=64,'tp'=2] {'tp'}, use_global_device_ids=true, to_apply=%region_6.7 | all-reduce | flops 16384 | bytes 65536 | tf_op jit(solution)/shard_map/psum | solution.py:168
  181.7 5.1 %all-to-all-done.6 = bf16[64,1,2,2048]{3,2,1,0:T(2,128)(2,1)S(1)} async-done(((bf16[64,1,2,2048]{3,2,1,0:T(2,128)(2,1)}), bf16[64,1,2,2048]{3,2,1,0:T(2,128)(2,1)S(1)}, u32[]{:S(2)}, u32[]{:S(2)}) %all-to-all-start.6) | async-done | bytes 524320 | tf_op jit(solution)/shard_map/all_to_all | solution.py:200
  187.0 0.8 fusion
  (132 shorter events, 15.0 us)
Async XLA Ops:
  0.6 15.8 %copy-start = (bf16[2048,512]{1,0:T(8,128)(2,1)S(1)}, bf16[2048,512]{1,0:T(8,128)(2,1)}, u32[]{:S(2)}) copy-start(bf16[2048,512]{1,0:T(8,128)(2,1)} %param.33) | copy-start | bytes 6291460
  4.1 12.8 %copy-start.26 = (f32[4,512]{1,0:T(4,128)S(1)}, f32[4,512]{1,0:T(4,128)}, u32[]{:S(2)}) copy-start(f32[4,512]{1,0:T(4,128)} %param.40) | copy-start | bytes 24580
  4.1 12.9 %copy-start.12 = (bf16[8,3,512]{2,0,1:T(8,128)(2,1)S(1)}, bf16[8,3,512]{2,0,1:T(8,128)(2,1)}, u32[]{:S(2)}) copy-start(bf16[8,3,512]{2,0,1:T(8,128)(2,1)} %param.43) | copy-start | bytes 73732
  4.1 12.9 %copy-start.27 = (f32[4,512]{1,0:T(4,128)S(1)}, f32[4,512]{1,0:T(4,128)}, u32[]{:S(2)}) copy-start(f32[4,512]{1,0:T(4,128)} %param.41) | copy-start | bytes 24580
  4.1 40.7 %all-to-all-start = ((bf16[64,8,2048]{2,1,0:T(8,128)(2,1)}), bf16[64,8,2048]{2,1,0:T(8,128)(2,1)}, u32[]{:S(2)}, u32[]{:S(2)}) async-start(bf16[64,8,2048]{2,1,0:T(8,128)(2,1)} %broadcast_in_dim.22), calls=%async_computation | async-start | bytes 4194304 | tf_op jit(solution)/shard_map/all_to_all | solution.py:15
  16.9 30.2 %copy-start.13 = (bf16[8,512]{1,0:T(8,128)(2,1)}, bf16[8,512]{1,0:T(8,128)(2,1)S(1)}, u32[]{:S(2)}) copy-start(bf16[8,512]{1,0:T(8,128)(2,1)S(1)} %convolution_convert_fusion.4) | copy-start | bytes 24580
  16.9 27.8 %copy-start.7 = (bf16[2048,1,32]{0,2,1:T(8,128)(2,1)S(1)}, bf16[2048,1,32]{0,2,1:T(8,128)(2,1)}, u32[]{:S(2)}) copy-start(bf16[2048,1,32]{0,2,1:T(8,128)(2,1)} %param.32) | copy-start | bytes 393220
  16.9 27.8 %copy-start.8 = (bf16[2048,1,32]{0,2,1:T(8,128)(2,1)S(1)}, bf16[2048,1,32]{0,2,1:T(8,128)(2,1)}, u32[]{:S(2)}) copy-start(bf16[2048,1,32]{0,2,1:T(8,128)(2,1)} %param.31) | copy-start | bytes 393220
  18.4 40.3 %copy-start.15 = (bf16[8,512]{1,0:T(8,128)(2,1)}, bf16[8,512]{1,0:T(8,128)(2,1)S(1)}, u32[]{:S(2)}) copy-start(bf16[8,512]{1,0:T(8,128)(2,1)S(1)} %convolution_convert_fusion.3) | copy-start | bytes 24580
  18.5 36.8 %copy-start.23 = (f32[4,2048]{1,0:T(4,128)S(1)}, f32[4,2048]{1,0:T(4,128)}, u32[]{:S(2)}) copy-start(f32[4,2048]{1,0:T(4,128)} %param.39) | copy-start | bytes 98308
  19.4 39.6 %copy-start.30 = (f32[32]{0:T(128)S(1)}, f32[32]{0:T(128)}, u32[]{:S(2)}) copy-start(f32[32]{0:T(128)} %param.45) | copy-start | bytes 388
  48.1 15.7 %all-to-all-start.1 = ((bf16[64,2,256]{2,1,0:T(2,128)(2,1)}), bf16[64,2,256]{2,1,0:T(2,128)(2,1)S(1)}, u32[]{:S(2)}, u32[]{:S(2)}) async-start(bf16[64,2,256]{2,1,0:T(2,128)(2,1)} %reshape.494), calls=%async_computation.1 | async-start | bytes 131072 | tf_op jit(solution)/shard_map/all_to_all | solution.py:128
  67.6 9.6 %copy-start.31 = (f32[32]{0:T(128)S(1)}, f32[32]{0:T(128)}, u32[]{:S(2)}) copy-start(f32[32]{0:T(128)} %param.45) | copy-start | bytes 388
  67.6 10.1 %copy-start.5 = (f32[8,2048]{1,0:T(8,128)S(1)}, f32[8,2048]{1,0:T(8,128)}, u32[]{:S(2)}) copy-start(f32[8,2048]{1,0:T(8,128)} %reshape.465) | copy-start | bytes 196612
  67.6 10.1 %copy-start.6 = (f32[8,2048]{1,0:T(8,128)S(1)}, f32[8,2048]{1,0:T(8,128)}, u32[]{:S(2)}) copy-start(f32[8,2048]{1,0:T(8,128)} %reshape.466) | copy-start | bytes 196612
  67.6 10.1 %copy-start.18 = (f32[1,2048]{1,0:T(1,128)S(1)}, f32[1,2048]{1,0:T(1,128)}, u32[]{:S(2)}) copy-start(f32[1,2048]{1,0:T(1,128)} %get-tuple-element.23) | copy-start | bytes 24580
  67.6 10.1 %copy-start.19 = (f32[1,2048]{1,0:T(1,128)S(1)}, f32[1,2048]{1,0:T(1,128)}, u32[]{:S(2)}) copy-start(f32[1,2048]{1,0:T(1,128)} %get-tuple-element.24) | copy-start | bytes 24580
  67.6 10.1 %copy-start.20 = (f32[1,2048]{1,0:T(1,128)S(1)}, f32[1,2048]{1,0:T(1,128)}, u32[]{:S(2)}) copy-start(f32[1,2048]{1,0:T(1,128)} %get-tuple-element.25) | copy-start | bytes 24580
  67.6 10.1 %copy-start.21 = (f32[1,2048]{1,0:T(1,128)S(1)}, f32[1,2048]{1,0:T(1,128)}, u32[]{:S(2)}) copy-start(f32[1,2048]{1,0:T(1,128)} %get-tuple-element.26) | copy-start | bytes 24580
  67.7 10.1 %copy-start.22 = (f32[2048]{0:T(1024)S(1)}, f32[2048]{0:T(1024)}, u32[]{:S(2)}) copy-start(f32[2048]{0:T(1024)} %mul.496) | copy-start | bytes 24580
  67.7 10.1 %copy-start.25 = (f32[2048]{0:T(1024)S(1)}, f32[2048]{0:T(1024)}, u32[]{:S(2)}) copy-start(f32[2048]{0:T(1024)} %param.46) | copy-start | bytes 24580
  79.4 6.7 %copy-start.29 = (f32[8,6]{1,0:T(8,128)S(1)}, f32[8,6]{1,0:T(8,128)}, u32[]{:S(2)}) copy-start(f32[8,6]{1,0:T(8,128)} %param.51) | copy-start | bytes 580
  79.4 34.0 %copy-start.9 = (bf16[2048,32]{0,1:T(8,128)(2,1)S(1)}, bf16[2048,32]{0,1:T(8,128)(2,1)}, u32[]{:S(2)}) copy-start(bf16[2048,32]{0,1:T(8,128)(2,1)} %param.47) | copy-start | bytes 393220
  79.4 34.0 %all-to-all-start.2 = ((bf16[64,8,2048]{2,1,0:T(8,128)(2,1)}), bf16[64,8,2048]{2,1,0:T(8,128)(2,1)}, u32[]{:S(2)}, u32[]{:S(2)}) async-start(bf16[64,8,2048]{2,1,0:T(8,128)(2,1)} %broadcast_in_dim.25), calls=%async_computation.2 | async-start | bytes 4194304 | tf_op jit(solution)/shard_map/all_to_all | solution.py:15
  86.2 50.9 %copy-start.3 = (bf16[8,2048]{1,0:T(8,128)(2,1)S(1)}, bf16[8,2048]{1,0:T(8,128)(2,1)}, u32[]{:S(2)}) copy-start(bf16[8,2048]{1,0:T(8,128)(2,1)} %param.29) | copy-start | bytes 98308
  86.2 51.0 %copy-start.17 = (f32[2048]{0:T(1024)S(1)}, f32[2048]{0:T(1024)}, u32[]{:S(2)}) copy-start(f32[2048]{0:T(1024)} %param.49) | copy-start | bytes 24580
  123.1 13.7 %all-to-all-start.3 = ((bf16[64,2,128]{2,1,0:T(2,128)(2,1)}), bf16[64,2,128]{2,1,0:T(2,128)(2,1)S(1)}, u32[]{:S(2)}, u32[]{:S(2)}) async-start(bf16[64,2,128]{2,1,0:T(2,128)(2,1)} %reshape.496), calls=%async_computation.3 | async-start | bytes 65536 | tf_op jit(solution)/shard_map/all_to_all | solution.py:161
  128.5 15.2 %copy-start.14 = (bf16[8,512]{1,0:T(8,128)(2,1)S(1)}, bf16[8,512]{1,0:T(8,128)(2,1)}, u32[]{:S(2)}) copy-start(bf16[8,512]{1,0:T(8,128)(2,1)} %copy-done.13) | copy-start | bytes 24580
  128.5 15.2 %copy-start.16 = (bf16[8,512]{1,0:T(8,128)(2,1)S(1)}, bf16[8,512]{1,0:T(8,128)(2,1)}, u32[]{:S(2)}) copy-start(bf16[8,512]{1,0:T(8,128)(2,1)} %copy-done.15) | copy-start | bytes 24580
  136.9 7.4 %copy-start.4 = (bf16[8,64,1,32]{1,3,2,0:T(8,128)(2,1)S(1)}, bf16[8,64,1,32]{1,3,2,0:T(8,128)(2,1)}, u32[]{:S(2)}) copy-start(bf16[8,64,1,32]{1,3,2,0:T(8,128)(2,1)} %get-tuple-element.17) | copy-start | bytes 98308
  138.8 16.1 %all-to-all-start.4 = ((bf16[64,1,2,2048]{3,2,1,0:T(2,128)(2,1)}), bf16[64,1,2,2048]{3,2,1,0:T(2,128)(2,1)S(1)}, u32[]{:S(2)}, u32[]{:S(2)}) async-start(bf16[64,1,2,2048]{3,2,1,0:T(2,128)(2,1)} %bitcast.35), calls=%async_computation.4 | async-start | bytes 1048576 | tf_op jit(solution)/shard_map/all_to_all | solution.py:194
  169.5 17.3 %all-to-all-start.6 = ((bf16[64,1,2,2048]{3,2,1,0:T(2,128)(2,1)}), bf16[64,1,2,2048]{3,2,1,0:T(2,128)(2,1)S(1)}, u32[]{:S(2)}, u32[]{:S(2)}) async-start(bf16[64,1,2,2048]{3,2,1,0:T(2,128)(2,1)} %copy.108), calls=%async_computation.6 | async-start | bytes 1048576 | tf_op jit(solution)/shard_map/all_to_all | solution.py:200
  (8 other events, 20.5 us)
where the time goes:
time: 189 us; the launch traced here: 188 us
  waiting for transfers between devices  79.6 us (42%)
  starting transfers between devices  40.5 us (21%)
  local copies, waits for them, and re-layouts  17.9 us (9%)
  blocking collectives  17.3 us (9%)
  other arithmetic  16.2 us (9%)
  matrix products  15 us (8%)
    all_to_all x2, waiting for transfers between devices, sent_to_all(): lax.all_to_all(jnp.broadcast_to(value[None], (size, *value.shape)), axis,...  52.6 us
    all_to_all x2, starting transfers between devices, sent_to_all(): lax.all_to_all(jnp.broadcast_to(value[None], (size, *value.shape)), axis,...  18.5 us
    all_to_all x1, waiting for transfers between devices, shards(): lax.all_to_all(outgoing, 'ep', split_axis=0, concat_axis=0, tiled=True)  9.58 us
    reduce_sum x1, other arithmetic, state_step(): jnp.sum(state_next * output_heads[:, :, None, :], axis=-1)  9.4 us
    all_to_all x1, waiting for transfers between devices, shards(): lax.all_to_all(summed_mix, 'ep', split_axis=0, concat_axis=1, tiled=True)  8.25 us
    all_to_all x1, starting transfers between devices, shards(): lax.all_to_all(projected, 'ep', split_axis=0, concat_axis=1, tiled=True)  7.22 us
    all_to_all x1, blocking collectives, sent_to_all(): lax.all_to_all(jnp.broadcast_to(value[None], (size, *value.shape)), axis,...  7.15 us
    psum x1, blocking collectives, shards(): summed_mix = lax.psum(partial_mix.astype(jnp.bfloat16), 'tp')  6.46 us
  transfers between devices with their start and end apart: 6, of which 6 were waited for; matrix products, arithmetic and copies ran while one was open for 6% of the time, Pallas kernels for 0%

commit v1 on v0

v1 whole, which is shorter than its diff:
```python
import functools

import jax
import jax.numpy as jnp
from jax import lax
from jax.experimental import pallas as pl
from jax.experimental.pallas import tpu as pltpu
from jax.sharding import PartitionSpec as P

MESH = pl.DeviceIdType.MESH
EPSILON = 1e-06
BF, F32 = jnp.bfloat16, jnp.float32
NT = (((1,), (1,)), ((), ()))
TN = (((0,), (0,)), ((), ()))
HALF = 1024
PIECES = ((0, 256), (256, 384), (640, 384))

SEM_A = 0
SEM_B = SEM_A + 48
SEM_F = SEM_B + 9
SEM_P = SEM_F + 3
SEM_W = SEM_P + 64
SEM_M = SEM_W + 3
SEM_Q = SEM_M + 16
SEM_X = SEM_Q + 32
SEM_Y = SEM_X + 64
SEM_FX = SEM_Y + 64
SEM_SH = SEM_FX + 1
SEM_YE = SEM_SH + 1
SEM_RF = SEM_YE + 1
SEM_COUNT = SEM_RF + 1

LOADED = (
    "tok", "g1", "wi", "wo", "wst", "sb", "dr", "eld", "vt", "it", "ot", "pv", "pi", "po", "hs",
    "gg", "g2", "routes", "cw", "rg", "ru", "rd", "cg", "cu", "cd", "st",
)


def silu(x):
    return x * (1.0 / (1.0 + jnp.exp(-x)))


def rms(x, gain):
    return x * lax.rsqrt(jnp.mean(x * x, axis=-1, keepdims=True) + EPSILON) * gain


def split_bf(x):
    hi = x.astype(BF)
    return hi, (x - hi.astype(F32)).astype(BF)


def dot(a, b, dims=(((1,), (0,)), ((), ()))):
    return lax.dot_general(a, b, dims, preferred_element_type=F32)


def lane_groups(pieces, lane):
    return jnp.where(
        lane < 32,
        pieces[0],
        jnp.where(lane < 64, pieces[1], jnp.where(lane < 96, pieces[2], pieces[3])),
    )


def layer_kernel(*refs):
    hbm = dict(zip(LOADED + ("gt", "vtp", "wmt"), refs[:29]))
    res_o, st_o, nv_o, ni_o, no_o = refs[29:34]
    v = dict(zip(LOADED, refs[34:60]))
    (
        X, WGV, WM, SP, R1, M, SQ, R2, SD, RX, XF, YS, YR, SY, RY, SHS, SHR, RES, RESR, DM, CM, QR,
        CC, FF, BV, DV, UT, ld, ss, rs,
    ) = refs[60:]

    e = lax.axis_index("ep")
    c = lax.axis_index("tp")
    oc = 1 - c
    z, y, x = e // 16, (e // 4) % 4, e % 4
    own = (z, y, x)

    def ep_of(zz, yy, xx):
        return zz * 16 + yy * 4 + xx

    def send(src, dst, so, ro, dev):
        return pltpu.make_async_remote_copy(
            src_ref=src, dst_ref=dst, send_sem=ss.at[so], recv_sem=rs.at[ro],
            device_id=dev, device_id_type=MESH,
        )

    def got(dst, ro):
        send(dst, dst, ro, ro, (e, oc)).wait_recv()

    def sent(src, so):
        send(src, src, so, so, (e, oc)).wait_send()

    pending = []

    def finish():
        for f in pending:
            f()

    loads = {}
    for k, n in enumerate(LOADED):
        loads[n] = pltpu.make_async_copy(hbm[n], v[n], ld.at[k])
    base = len(LOADED)
    gcopy = pltpu.make_async_copy(hbm["gt"], WGV.at[x], ld.at[base])
    vcopies = [
        pltpu.make_async_copy(hbm["vtp"], WGV.at[(x + 1 + j) % 4], ld.at[base + 1 + j])
        for j in range(3)
    ]
    wcopy = pltpu.make_async_copy(hbm["wmt"], WM.at[z], ld.at[base + 4])
    loads["tok"].start()
    loads["g1"].start()
    wcopy.start()
    loads["wst"].start()
    for n in ("wi", "wo", "sb", "dr", "eld", "vt", "it", "ot", "pv", "pi", "po", "hs", "gg", "g2", "routes", "cw"):
        loads[n].start()
    gcopy.start()
    for w in vcopies:
        w.start()
    for n in ("st", "cg", "cu", "cd", "rg", "ru", "rd"):
        loads[n].start()

    bar = pltpu.get_barrier_semaphore()
    pl.semaphore_signal(bar, inc=1, device_id=(e, oc), device_id_type=MESH)

    def sig_all(k, _):
        pl.semaphore_signal(
            bar, inc=1, device_id=(lax.rem(e + 1 + k, 64), c), device_id_type=MESH
        )
        return 0

    lax.fori_loop(0, 63, sig_all, 0)
    p_own = y * 4 + x

    def sig_plane(k, _):
        pl.semaphore_signal(
            bar, inc=1, device_id=(z * 16 + lax.rem(p_own + 1 + k, 16), oc), device_id_type=MESH
        )
        return 0

    lax.fori_loop(0, 15, sig_plane, 0)

    loads["tok"].wait()
    loads["g1"].wait()
    tok = v["tok"][...].astype(F32)
    normed = rms(tok, v["g1"][...]).astype(BF)
    nf = normed.astype(F32)
    X[c, z, y, x] = jnp.where(c == 0, nf[:, :HALF], nf[:, HALF:]).astype(BF)

    pl.semaphore_wait(bar, 79)

    def coords(i, line, p):
        a, b = p // 4, p % 4
        return ((line, a, b), (a, line, b), (a, b, line))[i]

    def plane_index(i):
        return (y * 4 + x, z * 4 + x, z * 4 + y)[i]

    def cols(i):
        return pl.ds(PIECES[i][0], PIECES[i][1])

    def own_piece(i):
        return X.at[c, z, y, x, :, cols(i)]

    def a_send(k, _):
        for i in range(3):
            p = plane_index(i)
            q = lax.rem(p + 1 + k, 16)
            dev = (ep_of(*coords(i, own[i], q)), c)
            send(own_piece(i), own_piece(i), SEM_A + i * 16 + q, SEM_A + i * 16 + p, dev).start()
        return 0

    lax.fori_loop(0, 15, a_send, 0)

    def a_sent(k, _):
        for i in range(3):
            q = lax.rem(plane_index(i) + 1 + k, 16)
            sent(own_piece(i), SEM_A + i * 16 + q)
        return 0

    pending.append(lambda: lax.fori_loop(0, 15, a_sent, 0))

    wcopy.wait()
    for d in range(1, 4):
        dev = (ep_of((z + d) % 4, y, x), c)
        send(WM.at[z], WM.at[z], SEM_W + d - 1, SEM_W + d - 1, dev).start()
        pending.append(lambda d=d: sent(WM.at[z], SEM_W + d - 1))

    for n in ("wi", "wo", "wst", "sb", "dr", "eld", "it", "ot", "pi", "po"):
        loads[n].wait()
    in_rows = dot(normed, v["wi"][...]).astype(BF)
    out_rows = dot(normed, v["wo"][...]).astype(BF)
    step_raw = dot(normed, v["wst"][...], NT)

    def conv(prior, fresh, taps):
        t = taps[...]
        total = fresh * t[3:4]
        for j in range(3):
            total = total + prior[j].astype(F32) * t[j : j + 1]
        return silu(total)

    b_conv = conv(v["pi"], in_rows.astype(F32), v["it"])
    c_conv = conv(v["po"], out_rows.astype(F32), v["ot"])
    BV[...] = b_conv
    pre = step_raw + v["sb"][...]
    dt = jnp.maximum(pre, 0.0) + jnp.log(1.0 + jnp.exp(-jnp.abs(pre)))
    dec = jnp.exp(-dt * v["dr"][...] + v["eld"][...])
    c_hi, c_lo = split_bf(c_conv)
    CC[...] = jnp.concatenate([c_hi.astype(F32), c_lo.astype(F32)], axis=0).astype(BF)

    def plane_of(i):
        if i == 0:
            return X.at[c, z, :, :, :, cols(i)]
        if i == 1:
            return X.at[c, :, y, :, :, cols(i)]
        return X.at[c, :, :, x, :, cols(i)]

    def plane_from(i, line):
        if i == 0:
            return X.at[c, line, :, :, :, cols(i)]
        if i == 1:
            return X.at[c, :, line, :, :, cols(i)]
        return X.at[c, :, :, line, :, cols(i)]

    def a_got(k, _):
        for i in range(3):
            q = lax.rem(plane_index(i) + 1 + k, 16)
            zz, yy, xx = coords(i, own[i], q)
            got(X.at[c, zz, yy, xx, :, cols(i)], SEM_A + i * 16 + q)
        return 0

    lax.fori_loop(0, 15, a_got, 0)
    for d in range(1, 4):
        for i in range(3):
            there = list(own)
            there[i] = (own[i] + d) % 4
            send(
                plane_of(i), plane_of(i), SEM_B + i * 3 + d - 1, SEM_B + i * 3 + d - 1,
                (ep_of(*there), c),
            ).start()
            pending.append(lambda i=i, d=d: sent(plane_of(i), SEM_B + i * 3 + d - 1))

    loads["st"].wait()
    row = lax.broadcasted_iota(jnp.int32, (8, 512), 0)
    QR[...] = jnp.zeros((8, 2048), F32)

    def q_step(b, _):
        for g in range(4):
            s = v["st"][b, g * 512 : (g + 1) * 512, :].astype(BF)
            r = dot(CC[:, g * 128 : (g + 1) * 128], s, NT)
            sl = pl.ds(g * 512, 512)
            QR[:, sl] = jnp.where(row == b, r[0:8] + r[8:16], QR[:, sl])
        return 0

    lax.fori_loop(0, 8, q_step, 0)

    d1 = dec.astype(BF)
    d2 = (dec - d1.astype(F32)).astype(BF)
    seq = lax.broadcasted_iota(jnp.int32, (8, 1024), 1) // 128
    ones = (seq == lax.broadcasted_iota(jnp.int32, (8, 1024), 0)).astype(BF)
    spread_dec = dot(d1, ones, TN) + dot(d2, ones, TN)
    for b in range(8):
        DV[b] = spread_dec[:, b * 128 : (b + 1) * 128]

    loads["hs"].wait()
    spread = (
        lax.broadcasted_iota(jnp.int32, (32, 2048), 1) // 64
        == lax.broadcasted_iota(jnp.int32, (32, 2048), 0)
    ).astype(BF)
    heads = jnp.concatenate([dt, dec, jnp.broadcast_to(v["hs"][...], (8, 32))], axis=0)
    h1 = heads.astype(BF)
    r1 = heads - h1.astype(F32)
    h2 = r1.astype(BF)
    h3 = (r1 - h2.astype(F32)).astype(BF)
    wide = dot(h1, spread) + dot(h2, spread) + dot(h3, spread)
    dt_w, dec_w, skip_w = wide[0:8], wide[8:16], wide[16:24]
    bc = b_conv * c_conv
    bc_w = jnp.concatenate(
        [
            jnp.broadcast_to(
                jnp.sum(bc[:, g * 128 : (g + 1) * 128], axis=1, keepdims=True), (8, 512)
            )
            for g in range(4)
        ],
        axis=1,
    )
    kept = dec_w * QR[...]
    v_gain = dt_w * bc_w + skip_w

    for i in range(3):
        for d in range(1, 4):
            got(plane_from(i, (own[i] + 4 - d) % 4), SEM_B + i * 3 + d - 1)
        send(
            X.at[c, :, :, :, :, cols(i)], X.at[c, :, :, :, :, cols(i)], SEM_F + i, SEM_F + i,
            (e, oc),
        ).start()
        pending.append(lambda i=i: sent(X.at[c, :, :, :, :, cols(i)], SEM_F + i))
    gcopy.wait()
    for w in vcopies:
        w.wait()
    for i in range(3):
        got(X.at[oc, :, :, :, :, cols(i)], SEM_F + i)
    proj = dot(
        X[0].reshape(512, HALF), WGV[:, :, :HALF].reshape(128, HALF), NT
    ) + dot(X[1].reshape(512, HALF), WGV[:, :, HALF:].reshape(128, HALF), NT)
    SP[...] = proj.reshape(64, 8, 128).astype(BF)

    def p_send(k, _):
        q = lax.rem(e + 1 + k, 64)
        send(SP.at[q], R1.at[e], SEM_P + q, SEM_P + e, (q, c)).start()
        return 0

    lax.fori_loop(0, 63, p_send, 0)

    def p_sent(k, _):
        q = lax.rem(e + 1 + k, 64)
        sent(SP.at[q], SEM_P + q)
        return 0

    pending.append(lambda: lax.fori_loop(0, 63, p_sent, 0))
    R1[e] = SP[e]

    loads["routes"].wait()
    loads["cw"].wait()
    lane8 = lax.broadcasted_iota(jnp.int32, (8, 128), 1)
    hit = jnp.zeros((8, 128), F32)
    wgt = jnp.zeros((8, 128), F32)
    rt = v["routes"][...]
    cwv = v["cw"][...]
    for k in range(6):
        eq = lane8 == rt[:, k : k + 1]
        hit = hit + jnp.where(eq, 1.0, 0.0)
        wgt = wgt + jnp.where(eq, cwv[:, k : k + 1], 0.0)
    before = (
        lax.broadcasted_iota(jnp.int32, (8, 8), 0) > lax.broadcasted_iota(jnp.int32, (8, 8), 1)
    ).astype(BF)
    slot = dot(before, hit.astype(BF))
    s0 = jnp.where(slot < 0.5, 1.0, 0.0)
    w1 = wgt.astype(BF).astype(F32)
    w2 = wgt - w1
    rows6 = jnp.concatenate(
        [hit * s0, hit * (1 - s0), w1 * s0, w1 * (1 - s0), w2 * s0, w2 * (1 - s0)], axis=0
    ).astype(BF)
    place = (
        lax.broadcasted_iota(jnp.int32, (128, 1024), 1) // 16
        == lax.broadcasted_iota(jnp.int32, (128, 1024), 0)
    ).astype(BF)
    six = dot(rows6, place)
    lane_r = lax.broadcasted_iota(jnp.int32, (8, 1024), 1)
    first = (lane_r // 8) % 2 == 0
    hsel = jnp.where(first, six[0:8], six[8:16])
    w1s = jnp.where(first, six[16:24], six[24:32])
    w2s = jnp.where(first, six[32:40], six[40:48])
    tile = lane_r % 8
    zero = jnp.zeros((8, 1024), F32)

    def diag(a):
        return jnp.concatenate([jnp.where(tile == j, a, zero) for j in range(8)], axis=0)

    DM[...] = jnp.concatenate([diag(hsel), jnp.zeros((64, 1024), F32)], axis=0).T.astype(BF)
    CM[...] = jnp.concatenate([diag(w1s), diag(w2s)], axis=0).astype(BF)
    for n in ("vt", "pv", "gg"):
        loads[n].wait()

    def p_got(k, _):
        q = lax.rem(e + 1 + k, 64)
        got(R1.at[q], SEM_P + q)
        return 0

    lax.fori_loop(0, 63, p_got, 0)

    gates, values = [], []
    for t in range(16):
        r = [R1[4 * t + j].astype(F32) for j in range(4)]
        gates.append(lane_groups(r, lane8))
        values.append(pltpu.roll(lane_groups([r[3], r[0], r[1], r[2]], lane8), 96, 1))
    gate = jnp.concatenate(gates, axis=1)
    value = jnp.concatenate(values, axis=1)
    value_rows = value.astype(BF)
    v_conv = conv(v["pv"], value, v["vt"])
    mixed = (kept + v_conv * v_gain) * silu(gate)
    normed_groups = []
    for g in range(4):
        m = mixed[:, g * 512 : (g + 1) * 512]
        normed_groups.append(m * lax.rsqrt(jnp.mean(m * m, axis=1, keepdims=True) + EPSILON))
    mixer_rows = jnp.concatenate(normed_groups, axis=1) * v["gg"][...]
    M[y, x] = mixer_rows.astype(BF)

    def m_send(k, _):
        q = lax.rem(p_own + 1 + k, 16)
        send(M.at[y, x], M.at[y, x], SEM_M + q, SEM_M + p_own, (z * 16 + q, c)).start()
        return 0

    lax.fori_loop(0, 15, m_send, 0)

    def m_sent(k, _):
        sent(M.at[y, x], SEM_M + lax.rem(p_own + 1 + k, 16))
        return 0

    pending.append(lambda: lax.fori_loop(0, 15, m_sent, 0))
    for new, old, fresh in ((nv_o, "pv", value_rows), (ni_o, "pi", in_rows), (no_o, "po", out_rows)):
        new[0] = v[old][1]
        new[1] = v[old][2]
        new[2] = fresh

    u = v_conv * dt_w
    u1 = u.astype(BF).astype(F32)
    pad = jnp.zeros((104, 2048), F32)
    UT[...] = jnp.concatenate([u1, u1, u - u1, pad], axis=0).T.astype(BF)

    def st_step(b, _):
        bv = BV[...]
        b1 = bv.astype(BF).astype(F32)
        keep = lax.broadcasted_iota(jnp.int32, (8, 512), 0) == b
        zero = jnp.zeros((8, 512), F32)
        k1, k2 = jnp.where(keep, b1, zero), jnp.where(keep, bv - b1, zero)
        rhs = jnp.concatenate([k1, k2, k1, jnp.zeros((104, 512), F32)], axis=0).astype(BF)
        for g in range(4):
            outer = dot(UT[g * 512 : (g + 1) * 512, :], rhs[:, g * 128 : (g + 1) * 128])
            for h in range(8):
                sl = pl.ds(g * 512 + h * 64, 64)
                keep_h = DV[b, pl.ds(g * 8 + h, 1), :]
                st_o[b, sl, :] = keep_h * v["st"][b, sl, :] + outer[h * 64 : (h + 1) * 64]
        return 0

    lax.fori_loop(0, 8, st_step, 0)
    for d in range(1, 4):
        got(WM.at[(z + 4 - d) % 4], SEM_W + d - 1)

    def m_got(k, _):
        q = lax.rem(p_own + 1 + k, 16)
        got(M.at[q // 4, q % 4], SEM_M + q)
        return 0

    lax.fori_loop(0, 15, m_got, 0)
    part = dot(M[...].reshape(128, 2048), WM[...].reshape(128, 2048), NT)
    SQ[...] = part.reshape(16, 8, 128).astype(BF)
    mine = c * 16 + p_own

    def q_send(k, _):
        q = lax.rem(p_own + 1 + k, 16)
        send(SQ.at[q], R2.at[mine], SEM_Q + q * 2 + c, SEM_Q + mine, (z * 16 + q, c)).start()
        send(SQ.at[q], R2.at[mine], SEM_Q + q * 2 + oc, SEM_Q + mine, (z * 16 + q, oc)).start()
        return 0

    send(SQ.at[p_own], R2.at[mine], SEM_Q + p_own * 2 + oc, SEM_Q + mine, (e, oc)).start()
    lax.fori_loop(0, 15, q_send, 0)

    def q_sent(k, _):
        q = lax.rem(p_own + 1 + k, 16)
        sent(SQ.at[q], SEM_Q + q * 2)
        sent(SQ.at[q], SEM_Q + q * 2 + 1)
        return 0

    pending.append(lambda: lax.fori_loop(0, 15, q_sent, 0))
    pending.append(lambda: sent(SQ.at[p_own], SEM_Q + p_own * 2 + oc))
    R2[mine] = SQ[p_own]

    def q_got(k, _):
        q = lax.rem(p_own + 1 + k, 16)
        got(R2.at[q], SEM_Q + q)
        got(R2.at[16 + q], SEM_Q + 16 + q)
        return 0

    got(R2.at[oc * 16 + p_own], SEM_Q + oc * 16 + p_own)
    lax.fori_loop(0, 15, q_got, 0)
    tiles = [None] * 16
    for yy in range(4):
        a = [
            (R2[yy * 4 + xx].astype(F32) + R2[16 + yy * 4 + xx].astype(F32)).astype(BF).astype(F32)
            for xx in range(4)
        ]
        for zz in range(4):
            moved = [
                a[xx] if xx == zz else pltpu.roll(a[xx], (32 * (xx - zz)) % 128, 1)
                for xx in range(4)
            ]
            tiles[zz * 4 + yy] = lane_groups(moved, lane8)
    mixed_out = jnp.concatenate(tiles, axis=1)
    loads["g2"].wait()
    stream = (tok + mixed_out).astype(BF).astype(F32)
    ffn = rms(stream, v["g2"][...]).astype(BF)
    ff32 = ffn.astype(F32)

    half = jnp.where(c == 0, ff32[:, :HALF], ff32[:, HALF:])
    stacked = jnp.concatenate([half[:, j * 128 : (j + 1) * 128] for j in range(8)], axis=0)
    FF[...] = jnp.concatenate([stacked, jnp.zeros((64, 128), F32)], axis=0).astype(BF)
    SD[...] = dot(DM[...], FF[...]).reshape(64, 16, 128).astype(BF)

    def x_send(k, _):
        q = lax.rem(e + 1 + k, 64)
        send(SD.at[q], RX.at[c, e], SEM_X + q, SEM_X + e, (q, c)).start()
        return 0

    lax.fori_loop(0, 63, x_send, 0)

    def x_sent(k, _):
        q = lax.rem(e + 1 + k, 64)
        sent(SD.at[q], SEM_X + q)
        return 0

    pending.append(lambda: lax.fori_loop(0, 63, x_sent, 0))
    RX[c, e] = SD[e]

    for n in ("cg", "cu", "cd"):
        loads[n].wait()
    sh = (silu(dot(ffn, v["cg"][...])) * dot(ffn, v["cu"][...])).astype(BF)
    shared = dot(sh, v["cd"][...]).astype(BF)
    SHS[...] = shared
    send(SHS, SHR, SEM_SH, SEM_SH, (e, oc)).start()
    pending.append(lambda: sent(SHS, SEM_SH))
    for n in ("rg", "ru", "rd"):
        loads[n].wait()

    def x_got(k, _):
        q = lax.rem(e + 1 + k, 64)
        got(RX.at[c, q], SEM_X + q)
        return 0

    lax.fori_loop(0, 63, x_got, 0)
    send(RX.at[c], RX.at[c], SEM_FX, SEM_FX, (e, oc)).start()
    pending.append(lambda: sent(RX.at[c], SEM_FX))
    got(RX.at[oc], SEM_FX)
    lhs = []
    for h in range(2):
        XF[...] = RX[h].astype(F32).reshape(1024, 128)
        for j in range(8):
            lhs.append(XF[pl.ds(j, 128, stride=8), :].astype(BF))
    rows = jnp.concatenate(lhs, axis=1)
    hid = (silu(dot(rows, v["rg"][...])) * dot(rows, v["ru"][...])).astype(BF)
    theirs = pl.ds(pl.multiple_of(oc * HALF, HALF), HALF)
    ours = pl.ds(pl.multiple_of(c * HALF, HALF), HALF)
    YS[...] = dot(hid, v["rd"][:, theirs]).astype(BF)
    send(YS, YR, SEM_YE, SEM_YE, (e, oc)).start()
    pending.append(lambda: sent(YS, SEM_YE))
    part_y = dot(hid, v["rd"][:, ours]).astype(BF).astype(F32)
    got(YR, SEM_YE)
    total_y = part_y + YR[...].astype(F32)
    for j in range(8):
        XF[pl.ds(j, 128, stride=8), :] = total_y[:, j * 128 : (j + 1) * 128]
    SY[...] = XF[...].reshape(64, 16, 128).astype(BF)

    def y_send(k, _):
        q = lax.rem(e + 1 + k, 64)
        send(SY.at[q], RY.at[e], SEM_Y + q, SEM_Y + e, (q, c)).start()
        return 0

    lax.fori_loop(0, 63, y_send, 0)

    def y_sent(k, _):
        q = lax.rem(e + 1 + k, 64)
        sent(SY.at[q], SEM_Y + q)
        return 0

    pending.append(lambda: lax.fori_loop(0, 63, y_sent, 0))
    RY[e] = SY[e]
    got(SHR, SEM_SH)
    resid = stream + (shared.astype(F32) + SHR[...].astype(F32))
    resid_half = jnp.where(c == 0, resid[:, :HALF], resid[:, HALF:])

    def y_got(k, _):
        q = lax.rem(e + 1 + k, 64)
        got(RY.at[q], SEM_Y + q)
        return 0

    lax.fori_loop(0, 63, y_got, 0)
    both = dot(CM[...], RY[...].reshape(1024, 128))
    comb = both[0:64] + both[64:128]
    routed = jnp.concatenate([comb[j * 8 : (j + 1) * 8] for j in range(8)], axis=1)
    res = (resid_half + routed).astype(BF)
    RES[...] = res
    send(RES, RESR, SEM_RF, SEM_RF, (e, oc)).start()
    pending.append(lambda: sent(RES, SEM_RF))
    res_o[:, ours] = res
    got(RESR, SEM_RF)
    res_o[:, theirs] = RESR[...]
    finish()


def store_kernel(*refs):
    n = len(refs) // 2
    sem = refs[-1]
    copies = []
    for k in range(n):
        src, dst = refs[k], refs[n + k]
        if k == 1:
            copies += [(src.at[b], dst.at[b]) for b in range(8)]
        else:
            copies.append((src, dst))
    started = [pltpu.make_async_copy(a, b, sem.at[k]) for k, (a, b) in enumerate(copies)]
    for w in started:
        w.start()
    for w in started:
        w.wait()


def shards(
    tokens,
    mixer_norm_gain,
    gate_projection_weight,
    value_projection_weight,
    input_projection_weight,
    output_projection_weight,
    step_projection_weight,
    head_step_bias,
    head_decay_rate,
    extra_log_decay,
    value_taps,
    input_taps,
    output_taps,
    prior_values,
    prior_input_maps,
    prior_output_maps,
    head_skip_gain,
    group_norm_gain,
    mixer_output_weight,
    recurrent_state,
    expert_norm_gain,
    routes,
    chosen_expert_weight,
    routed_gate_weight,
    routed_up_weight,
    routed_down_weight,
    common_gate_weight,
    common_up_weight,
    common_down_weight,
):
    pv, pi, po = (
        jnp.transpose(a, (1, 0, 2)) for a in (prior_values, prior_input_maps, prior_output_maps)
    )
    state = recurrent_state.reshape(8, 2048, 128)
    vals = dict(
        tok=tokens,
        g1=mixer_norm_gain[None],
        wi=input_projection_weight,
        wo=output_projection_weight,
        wst=step_projection_weight.T,
        sb=head_step_bias[None],
        dr=head_decay_rate[None],
        eld=extra_log_decay,
        vt=value_taps,
        it=input_taps,
        ot=output_taps,
        pv=pv,
        pi=pi,
        po=po,
        hs=head_skip_gain[None],
        gg=group_norm_gain[None],
        g2=expert_norm_gain[None],
        routes=routes,
        cw=chosen_expert_weight,
        rg=routed_gate_weight[0],
        ru=routed_up_weight[0],
        rd=routed_down_weight[0],
        cg=common_gate_weight,
        cu=common_up_weight,
        cd=common_down_weight,
        st=state,
    )
    ins = [vals[n] for n in LOADED] + [
        jnp.transpose(gate_projection_weight, (1, 2, 0))[0],
        jnp.transpose(value_projection_weight, (1, 2, 0))[0],
        mixer_output_weight.T,
    ]
    vm = pltpu.VMEM
    scratch = [vm(vals[n].shape, vals[n].dtype) for n in LOADED] + [
        vm((2, 4, 4, 4, 8, HALF), BF),
        vm((4, 32, 2048), BF),
        vm((4, 32, 2048), BF),
        vm((64, 8, 128), BF),
        vm((64, 8, 128), BF),
        vm((4, 4, 8, 2048), BF),
        vm((16, 8, 128), BF),
        vm((32, 8, 128), BF),
        vm((64, 16, 128), BF),
        vm((2, 64, 16, 128), BF),
        vm((1024, 128), F32),
        vm((128, HALF), BF),
        vm((128, HALF), BF),
        vm((64, 16, 128), BF),
        vm((64, 16, 128), BF),
        vm((8, 2048), BF),
        vm((8, 2048), BF),
        vm((8, HALF), BF),
        vm((8, HALF), BF),
        vm((1024, 128), BF),
        vm((128, 1024), BF),
        vm((8, 2048), F32),
        vm((16, 512), BF),
        vm((128, 128), BF),
        vm((8, 512), F32),
        vm((8, 32, 128), F32),
        vm((2048, 128), BF),
        pltpu.SemaphoreType.DMA((len(LOADED) + 5,)),
        pltpu.SemaphoreType.DMA((SEM_COUNT,)),
        pltpu.SemaphoreType.DMA((SEM_COUNT,)),
    ]
    shapes = [
        ((8, 2048), BF),
        ((8, 2048, 128), F32),
        ((3, 8, 2048), BF),
        ((3, 8, 512), BF),
        ((3, 8, 512), BF),
    ]
    held = pl.pallas_call(
        layer_kernel,
        out_shape=[pltpu.VMEM(a, t) for a, t in shapes],
        in_specs=[pl.BlockSpec(memory_space=pltpu.HBM)] * len(ins),
        out_specs=[pl.BlockSpec(memory_space=pltpu.VMEM)] * 5,
        scratch_shapes=scratch,
        compiler_params=pltpu.CompilerParams(
            collective_id=0, has_side_effects=True, vmem_limit_bytes=50 * 2**20
        ),
    )(*ins)
    result, state_next, nv, ni, no = pl.pallas_call(
        store_kernel,
        out_shape=[jax.ShapeDtypeStruct(a, t) for a, t in shapes],
        in_specs=[pl.BlockSpec(memory_space=pl.ANY)] * 5,
        out_specs=[pl.BlockSpec(memory_space=pltpu.HBM)] * 5,
        scratch_shapes=[pltpu.SemaphoreType.DMA((12,))],
        compiler_params=pltpu.CompilerParams(vmem_limit_bytes=2**20),
    )(*held)
    return (
        result,
        state_next.reshape(8, 32, 64, 128),
        jnp.transpose(nv, (1, 0, 2)),
        jnp.transpose(ni, (1, 0, 2)),
        jnp.transpose(no, (1, 0, 2)),
    )


def solution(mesh):
    return jax.shard_map(
        shards,
        mesh=mesh,
        in_specs=(
            P("ep", None),
            P(),
            P(None, "tp", "ep"),
            P(None, "tp", "ep"),
            P(None, "tp"),
            P(None, "tp"),
            P(None, "tp"),
            P("tp"),
            P("tp"),
            P("ep", "tp"),
            P(None, "tp"),
            P(None, "tp"),
            P(None, "tp"),
            P("ep", None, "tp"),
            P("ep", None, "tp"),
            P("ep", None, "tp"),
            P("tp"),
            P("tp"),
            P("tp", "ep"),
            P("ep", "tp", None, None),
            P(),
            P("ep", None),
            P("ep", None),
            P("ep", None, "tp"),
            P("ep", None, "tp"),
            P("ep", "tp", None),
            P(None, "tp"),
            P(None, "tp"),
            P("tp", None),
        ),
        out_specs=(
            P("ep", None),
            P("ep", "tp", None, None),
            P("ep", None, "tp"),
            P("ep", None, "tp"),
            P("ep", None, "tp"),
        ),
        check_vma=False,
    )
```

time: 189 us -> 80.7 us (0.43)
  Pallas kernels: 0 us -> 79.9 us
  waiting for transfers between devices: 79.6 us -> 0 us
  starting transfers between devices: 40.5 us -> 0 us
  local copies, waits for them, and re-layouts: 17.9 us -> 0 us
  blocking collectives: 17.3 us -> 0 us
  other arithmetic: 16.2 us -> 0 us
  matrix products: 15 us -> 0 us
    pallas_call x0 -> x2, Pallas kernels: none -> 79.9 us  [the longest x1 76.5 us: shards(): pl.pallas_call(layer_kernel, out_shape=[pltpu.VMEM(a, t) for a, t in shap...]
    all_to_all x6 -> x0, waiting for transfers between devices: 79.6 us -> none  [the longest x2 52.6 us: sent_to_all(): lax.all_to_all(jnp.broadcast_to(value[None], (size, *value.shape)), axis,...]
    all_to_all x6 -> x0, starting transfers between devices: 40.5 us -> none  [the longest x2 18.5 us: sent_to_all(): lax.all_to_all(jnp.broadcast_to(value[None], (size, *value.shape)), axis,...]
    dot_general x11 -> x0, matrix products: 15 us -> none  [the longest x1 2.35 us: shards(): jnp.dot(gather_directly(normed, 'ep', 0), both_pieces, preferred_element_...]
    reduce_sum x8 -> x0, other arithmetic: 12.2 us -> none  [the longest x1 9.4 us: state_step(): jnp.sum(state_next * output_heads[:, :, None, :], axis=-1)]
    psum x2 -> x0, blocking collectives: 10.2 us -> none  [the longest x1 6.46 us: shards(): summed_mix = lax.psum(partial_mix.astype(jnp.bfloat16), 'tp')]
    all_to_all x1 -> x0, blocking collectives: 7.15 us -> none  [sent_to_all(): lax.all_to_all(jnp.broadcast_to(value[None], (size, *value.shape)), axis,...]
    mul x8 -> x0, local copies, waits for them, and re-layouts: 3.54 us -> none  [the longest x3 2.03 us: short_conv(): summed = summed + window[:, offset].astype(jnp.float32) * weight[offset]]
  transfers between devices with their start and end apart: 6 -> 0, of which waited for: 6 -> 0; matrix products, arithmetic and copies ran while one was open for 6% -> 0% of each run, Pallas kernels for 0% -> 0%
where the time goes in v1:
time: 80.7 us; the launch traced here: 80.6 us
  Pallas kernels  79.9 us (99%)
    pallas_call x1, Pallas kernels, shards(): pl.pallas_call(layer_kernel, out_shape=[pltpu.VMEM(a, t) for a, t in shap...  76.5 us
    pallas_call x1, Pallas kernels, shards(): pl.pallas_call(store_kernel, out_shape=[jax.ShapeDtypeStruct(a, t) for a,...  3.42 us

profile of v1, /device:TPU:1, one launch (start us, length us, event | category | flops | bytes accessed | tf_op | source)
XLA Modules:
  0.0 80.6 jit_solution(17448913051113829915)
XLA Ops:
  0.6 76.5 %shard_map.308 = (bf16[8,2048]{1,0:T(8,128)(2,1)S(1)}, f32[8,2048,128]{2,1,0:T(8,128)S(1)}, bf16[3,8,2048]{2,1,0:T(8,128)(2,1)S(1)}, bf16[3,8,512]{2,1,0:T(8,128)(2,1)S(1)}, bf16[3,8,512]{2,1,0:T(8,128)(2,1)S(1)}) custom-call(bf16[8,2048]{1,0:T(8,128)(2,1)} %refs_0_.1, f32[1,2048]{1,0:T(1,128)} %bitcast.36, bf16[2048,512]{1,0:T(8,128)(2,1)} %refs_2_.1, ...), custom_call_target="tpu_custom_call" | custom-call | tf_op jit(solution)/shard_map/pallas_call | solution.py:704
  77.2 3.4 %shard_map.309 = (bf16[8,2048]{1,0:T(8,128)(2,1)}, f32[8,2048,128]{2,1,0:T(8,128)}, bf16[3,8,2048]{2,1,0:T(8,128)(2,1)}, bf16[3,8,512]{2,1,0:T(8,128)(2,1)}, bf16[3,8,512]{2,1,0:T(8,128)(2,1)}) custom-call(bf16[8,2048]{1,0:T(8,128)(2,1)S(1)} %get-tuple-element.15.refs_0_, f32[8,2048,128]{2,1,0:T(8,128)S(1)} %get-tuple-element.16.refs_1_, ...), custom_call_target="tpu_custom_call" | custom-call | tf_op jit(solution)/shard_map/pallas_call | solution.py:714

commit v2 on v1

--- a/solution.py
+++ b/solution.py
@@ -17,8 +17,8 @@
 
 SEM_A = 0
 SEM_B = SEM_A + 48
-SEM_F = SEM_B + 9
-SEM_P = SEM_F + 3
+SEM_F = SEM_B + 18
+SEM_P = SEM_F + 12
 SEM_W = SEM_P + 64
 SEM_M = SEM_W + 3
 SEM_Q = SEM_M + 16
@@ -30,6 +30,15 @@
 SEM_RF = SEM_YE + 1
 SEM_COUNT = SEM_RF + 1
 
+def hops(d):
+    return sum(min(k, 4 - k) for k in d)
+
+
+FAR = sorted(
+    [(i // 16, i // 4 % 4, i % 4) for i in range(1, 64)], key=hops, reverse=True
+)
+FAR_PLANE = sorted([(i // 4, i % 4) for i in range(1, 16)], key=hops, reverse=True)
+
 LOADED = (
     "tok", "g1", "wi", "wo", "wst", "sb", "dr", "eld", "vt", "it", "ot", "pv", "pi", "po", "hs",
     "gg", "g2", "routes", "cw", "rg", "ru", "rd", "cg", "cu", "cd", "st",
@@ -96,6 +105,7 @@
     def finish():
         for f in pending:
             f()
+        pending.clear()
 
     loads = {}
     for k, n in enumerate(LOADED):
@@ -122,22 +132,19 @@
     bar = pltpu.get_barrier_semaphore()
     pl.semaphore_signal(bar, inc=1, device_id=(e, oc), device_id_type=MESH)
 
-    def sig_all(k, _):
-        pl.semaphore_signal(
-            bar, inc=1, device_id=(lax.rem(e + 1 + k, 64), c), device_id_type=MESH
-        )
-        return 0
-
-    lax.fori_loop(0, 63, sig_all, 0)
+    zs, ys, xs = ([(w + d) % 4 for d in range(4)] for w in own)
+
+    def peer(d):
+        return zs[d[0]] * 16 + ys[d[1]] * 4 + xs[d[2]]
+
     p_own = y * 4 + x
 
-    def sig_plane(k, _):
-        pl.semaphore_signal(
-            bar, inc=1, device_id=(z * 16 + lax.rem(p_own + 1 + k, 16), oc), device_id_type=MESH
-        )
-        return 0
-
-    lax.fori_loop(0, 15, sig_plane, 0)
+    def plane_peer(d):
+        return ys[d[0]] * 4 + xs[d[1]]
+
+    greeted = [d for d in FAR if 0 in d]
+    for d in greeted:
+        pl.semaphore_signal(bar, inc=1, device_id=(peer(d), c), device_id_type=MESH)
 
     loads["tok"].wait()
     loads["g1"].wait()
@@ -146,7 +153,7 @@
     nf = normed.astype(F32)
     X[c, z, y, x] = jnp.where(c == 0, nf[:, :HALF], nf[:, HALF:]).astype(BF)
 
-    pl.semaphore_wait(bar, 79)
+    pl.semaphore_wait(bar, 1 + len(greeted))
 
     def coords(i, line, p):
         a, b = p // 4, p % 4
@@ -207,19 +214,30 @@
     c_hi, c_lo = split_bf(c_conv)
     CC[...] = jnp.concatenate([c_hi.astype(F32), c_lo.astype(F32)], axis=0).astype(BF)
 
-    def plane_of(i):
+    def plane(i, line, h=None):
+        part = slice(None) if h is None else pl.ds(2 * h, 2)
         if i == 0:
-            return X.at[c, z, :, :, :, cols(i)]
+            return X.at[c, line, part, :, :, cols(i)]
         if i == 1:
-            return X.at[c, :, y, :, :, cols(i)]
-        return X.at[c, :, :, x, :, cols(i)]
-
-    def plane_from(i, line):
-        if i == 0:
-            return X.at[c, line, :, :, :, cols(i)]
-        if i == 1:
-            return X.at[c, :, line, :, :, cols(i)]
-        return X.at[c, :, :, line, :, cols(i)]
+            return X.at[c, part, line, :, :, cols(i)]
+        return X.at[c, part, :, line, :, cols(i)]
+
+    def line_peer(i, d):
+        there = list(own)
+        there[i] = (own[i] + d) % 4
+        return (ep_of(*there), c)
+
+    def line_send(i, line, h, d, k):
+        src = plane(i, line, h)
+        k = SEM_B + i * 6 + k
+        send(src, src, k, k, line_peer(i, d)).start()
+        pending.append(lambda: sent(plane(i, line, h), k))
+
+    def hand_over(i, d):
+        line = (own[i] + d) % 4
+        k = SEM_F + i * 4 + d
+        send(plane(i, line), plane(i, line), k, k, (e, oc)).start()
+        pending.append(lambda: sent(plane(i, line), k))
 
     def a_got(k, _):
         for i in range(3):
@@ -229,15 +247,11 @@
         return 0
 
     lax.fori_loop(0, 15, a_got, 0)
-    for d in range(1, 4):
+    for k, (h, d) in enumerate(((0, 1), (1, 3), (1, 1), (0, 3))):
         for i in range(3):
-            there = list(own)
-            there[i] = (own[i] + d) % 4
-            send(
-                plane_of(i), plane_of(i), SEM_B + i * 3 + d - 1, SEM_B + i * 3 + d - 1,
-                (ep_of(*there), c),
-            ).start()
-            pending.append(lambda i=i, d=d: sent(plane_of(i), SEM_B + i * 3 + d - 1))
+            line_send(i, own[i], h, d, k)
+    for i in range(3):
+        hand_over(i, 0)
 
     loads["st"].wait()
     row = lax.broadcasted_iota(jnp.int32, (8, 512), 0)
@@ -287,29 +301,46 @@
     v_gain = dt_w * bc_w + skip_w
 
     for i in range(3):
-        for d in range(1, 4):
-            got(plane_from(i, (own[i] + 4 - d) % 4), SEM_B + i * 3 + d - 1)
-        send(
-            X.at[c, :, :, :, :, cols(i)], X.at[c, :, :, :, :, cols(i)], SEM_F + i, SEM_F + i,
-            (e, oc),
-        ).start()
-        pending.append(lambda i=i: sent(X.at[c, :, :, :, :, cols(i)], SEM_F + i))
+        before, after = (own[i] + 3) % 4, (own[i] + 1) % 4
+        got(plane(i, before, 0), SEM_B + i * 6)
+        line_send(i, before, 0, 1, 4)
+        got(plane(i, after, 1), SEM_B + i * 6 + 1)
+        line_send(i, after, 1, 3, 5)
+    for i in range(3):
+        before, after = (own[i] + 3) % 4, (own[i] + 1) % 4
+        got(plane(i, before, 1), SEM_B + i * 6 + 2)
+        hand_over(i, 3)
+        got(plane(i, after, 0), SEM_B + i * 6 + 3)
+        hand_over(i, 1)
+    for i in range(3):
+        across = (own[i] + 2) % 4
+        got(plane(i, across, 0), SEM_B + i * 6 + 4)
+        got(plane(i, across, 1), SEM_B + i * 6 + 5)
+        hand_over(i, 2)
     gcopy.wait()
     for w in vcopies:
         w.wait()
+    proj = jnp.zeros((512, 128), F32)
     for i in range(3):
-        got(X.at[oc, :, :, :, :, cols(i)], SEM_F + i)
-    proj = dot(
-        X[0].reshape(512, HALF), WGV[:, :, :HALF].reshape(128, HALF), NT
-    ) + dot(X[1].reshape(512, HALF), WGV[:, :, HALF:].reshape(128, HALF), NT)
+        for d in range(4):
+            line = (own[i] + d) % 4
+            view = X.at[oc]
+            if i == 0:
+                view = view.at[line, :, :, :, cols(i)]
+            elif i == 1:
+                view = view.at[:, line, :, :, cols(i)]
+            else:
+                view = view.at[:, :, line, :, cols(i)]
+            got(view, SEM_F + i * 4 + d)
+        at, width = PIECES[i]
+        for h in range(2):
+            w = WGV[:, :, h * HALF + at : h * HALF + at + width].reshape(128, width)
+            proj = proj + dot(X[h, :, :, :, :, at : at + width].reshape(512, width), w, NT)
     SP[...] = proj.reshape(64, 8, 128).astype(BF)
 
-    def p_send(k, _):
-        q = lax.rem(e + 1 + k, 64)
+    for d in FAR:
+        q = peer(d)
         send(SP.at[q], R1.at[e], SEM_P + q, SEM_P + e, (q, c)).start()
-        return 0
-
-    lax.fori_loop(0, 63, p_send, 0)
 
     def p_sent(k, _):
         q = lax.rem(e + 1 + k, 64)
@@ -361,12 +392,9 @@
     for n in ("vt", "pv", "gg"):
         loads[n].wait()
 
-    def p_got(k, _):
-        q = lax.rem(e + 1 + k, 64)
+    for d in FAR[::-1]:
+        q = peer(d)
         got(R1.at[q], SEM_P + q)
-        return 0
-
-    lax.fori_loop(0, 63, p_got, 0)
 
     gates, values = [], []
     for t in range(16):
@@ -385,12 +413,9 @@
     mixer_rows = jnp.concatenate(normed_groups, axis=1) * v["gg"][...]
     M[y, x] = mixer_rows.astype(BF)
 
-    def m_send(k, _):
-        q = lax.rem(p_own + 1 + k, 16)
+    for d in FAR_PLANE:
+        q = plane_peer(d)
         send(M.at[y, x], M.at[y, x], SEM_M + q, SEM_M + p_own, (z * 16 + q, c)).start()
-        return 0
-
-    lax.fori_loop(0, 15, m_send, 0)
 
     def m_sent(k, _):
         sent(M.at[y, x], SEM_M + lax.rem(p_own + 1 + k, 16))
@@ -423,6 +448,7 @@
         return 0
 
     lax.fori_loop(0, 8, st_step, 0)
+    finish()
     for d in range(1, 4):
         got(WM.at[(z + 4 - d) % 4], SEM_W + d - 1)
 
@@ -436,14 +462,11 @@
     SQ[...] = part.reshape(16, 8, 128).astype(BF)
     mine = c * 16 + p_own
 
-    def q_send(k, _):
-        q = lax.rem(p_own + 1 + k, 16)
+    for d in FAR_PLANE:
+        q = plane_peer(d)
+        send(SQ.at[q], R2.at[mine], SEM_Q + q * 2 + oc, SEM_Q + mine, (z * 16 + q, oc)).start()
         send(SQ.at[q], R2.at[mine], SEM_Q + q * 2 + c, SEM_Q + mine, (z * 16 + q, c)).start()
-        send(SQ.at[q], R2.at[mine], SEM_Q + q * 2 + oc, SEM_Q + mine, (z * 16 + q, oc)).start()
-        return 0
-
     send(SQ.at[p_own], R2.at[mine], SEM_Q + p_own * 2 + oc, SEM_Q + mine, (e, oc)).start()
-    lax.fori_loop(0, 15, q_send, 0)
 
     def q_sent(k, _):
         q = lax.rem(p_own + 1 + k, 16)
@@ -486,12 +509,9 @@
     FF[...] = jnp.concatenate([stacked, jnp.zeros((64, 128), F32)], axis=0).astype(BF)
     SD[...] = dot(DM[...], FF[...]).reshape(64, 16, 128).astype(BF)
 
-    def x_send(k, _):
-        q = lax.rem(e + 1 + k, 64)
+    for d in FAR:
+        q = peer(d)
         send(SD.at[q], RX.at[c, e], SEM_X + q, SEM_X + e, (q, c)).start()
-        return 0
-
-    lax.fori_loop(0, 63, x_send, 0)
 
     def x_sent(k, _):
         q = lax.rem(e + 1 + k, 64)
@@ -511,12 +531,9 @@
     for n in ("rg", "ru", "rd"):
         loads[n].wait()
 
-    def x_got(k, _):
-        q = lax.rem(e + 1 + k, 64)
+    for d in FAR[::-1]:
+        q = peer(d)
         got(RX.at[c, q], SEM_X + q)
-        return 0
-
-    lax.fori_loop(0, 63, x_got, 0)
     send(RX.at[c], RX.at[c], SEM_FX, SEM_FX, (e, oc)).start()
     pending.append(lambda: sent(RX.at[c], SEM_FX))
     got(RX.at[oc], SEM_FX)
@@ -539,12 +556,9 @@
         XF[pl.ds(j, 128, stride=8), :] = total_y[:, j * 128 : (j + 1) * 128]
     SY[...] = XF[...].reshape(64, 16, 128).astype(BF)
 
-    def y_send(k, _):
-        q = lax.rem(e + 1 + k, 64)
+    for d in FAR:
+        q = peer(d)
         send(SY.at[q], RY.at[e], SEM_Y + q, SEM_Y + e, (q, c)).start()
-        return 0
-
-    lax.fori_loop(0, 63, y_send, 0)
 
     def y_sent(k, _):
         q = lax.rem(e + 1 + k, 64)
@@ -557,12 +571,11 @@
     resid = stream + (shared.astype(F32) + SHR[...].astype(F32))
     resid_half = jnp.where(c == 0, resid[:, :HALF], resid[:, HALF:])
 
-    def y_got(k, _):
-        q = lax.rem(e + 1 + k, 64)
+    while len(pending) > 1:
+        pending.pop(0)()
+    for d in FAR[::-1]:
+        q = peer(d)
         got(RY.at[q], SEM_Y + q)
-        return 0
-
-    lax.fori_loop(0, 63, y_got, 0)
     both = dot(CM[...], RY[...].reshape(1024, 128))
     comb = both[0:64] + both[64:128]
     routed = jnp.concatenate([comb[j * 8 : (j + 1) * 8] for j in range(8)], axis=1)

time: 80.7 us -> 74.5 us (0.923)
  Pallas kernels: 79.9 us -> 73.7 us
    pallas_call x1, Pallas kernels: 76.5 us -> 70.3 us  [shards(): pl.pallas_call(layer_kernel, out_shape=[pltpu.VMEM(a, t) for a, t in shap...]
where the time goes in v2:
time: 74.5 us; the launch traced here: 74.4 us
  Pallas kernels  73.7 us (99%)
    pallas_call x1, Pallas kernels, shards(): pl.pallas_call(layer_kernel, out_shape=[pltpu.VMEM(a, t) for a, t in shap...  70.3 us
    pallas_call x1, Pallas kernels, shards(): pl.pallas_call(store_kernel, out_shape=[jax.ShapeDtypeStruct(a, t) for a,...  3.42 us

profile of v2, /device:TPU:1, one launch (start us, length us, event | category | flops | bytes accessed | tf_op | source)
XLA Modules:
  0.0 74.4 jit_solution(16997962870946664556)
XLA Ops:
  0.6 70.3 %shard_map.308 = (bf16[8,2048]{1,0:T(8,128)(2,1)S(1)}, f32[8,2048,128]{2,1,0:T(8,128)S(1)}, bf16[3,8,2048]{2,1,0:T(8,128)(2,1)S(1)}, bf16[3,8,512]{2,1,0:T(8,128)(2,1)S(1)}, bf16[3,8,512]{2,1,0:T(8,128)(2,1)S(1)}) custom-call(bf16[8,2048]{1,0:T(8,128)(2,1)} %refs_0_.1, f32[1,2048]{1,0:T(1,128)} %bitcast.36, bf16[2048,512]{1,0:T(8,128)(2,1)} %refs_2_.1, ...), custom_call_target="tpu_custom_call" | custom-call | tf_op jit(solution)/shard_map/pallas_call | solution.py:717
  71.0 3.4 %shard_map.309 = (bf16[8,2048]{1,0:T(8,128)(2,1)}, f32[8,2048,128]{2,1,0:T(8,128)}, bf16[3,8,2048]{2,1,0:T(8,128)(2,1)}, bf16[3,8,512]{2,1,0:T(8,128)(2,1)}, bf16[3,8,512]{2,1,0:T(8,128)(2,1)}) custom-call(bf16[8,2048]{1,0:T(8,128)(2,1)S(1)} %get-tuple-element.15.refs_0_, f32[8,2048,128]{2,1,0:T(8,128)S(1)} %get-tuple-element.16.refs_1_, ...), custom_call_target="tpu_custom_call" | custom-call | tf_op jit(solution)/shard_map/pallas_call | solution.py:727

commit v3 on v2

--- a/solution.py
+++ b/solution.py
@@ -20,12 +20,12 @@
 SEM_F = SEM_B + 18
 SEM_P = SEM_F + 12
 SEM_W = SEM_P + 64
-SEM_M = SEM_W + 3
-SEM_Q = SEM_M + 16
-SEM_X = SEM_Q + 32
+SEM_M = SEM_W + 16
+SEM_Q = SEM_M + 4
+SEM_X = SEM_Q + 8
 SEM_Y = SEM_X + 64
 SEM_FX = SEM_Y + 64
-SEM_SH = SEM_FX + 1
+SEM_SH = SEM_FX + 4
 SEM_YE = SEM_SH + 1
 SEM_RF = SEM_YE + 1
 SEM_COUNT = SEM_RF + 1
@@ -37,7 +37,6 @@
 FAR = sorted(
     [(i // 16, i // 4 % 4, i % 4) for i in range(1, 64)], key=hops, reverse=True
 )
-FAR_PLANE = sorted([(i // 4, i % 4) for i in range(1, 16)], key=hops, reverse=True)
 
 LOADED = (
     "tok", "g1", "wi", "wo", "wst", "sb", "dr", "eld", "vt", "it", "ot", "pv", "pi", "po", "hs",
@@ -116,7 +115,7 @@
         pltpu.make_async_copy(hbm["vtp"], WGV.at[(x + 1 + j) % 4], ld.at[base + 1 + j])
         for j in range(3)
     ]
-    wcopy = pltpu.make_async_copy(hbm["wmt"], WM.at[z], ld.at[base + 4])
+    wcopy = pltpu.make_async_copy(hbm["wmt"], WM.at[z, y], ld.at[base + 4])
     loads["tok"].start()
     loads["g1"].start()
     wcopy.start()
@@ -137,11 +136,6 @@
     def peer(d):
         return zs[d[0]] * 16 + ys[d[1]] * 4 + xs[d[2]]
 
-    p_own = y * 4 + x
-
-    def plane_peer(d):
-        return ys[d[0]] * 4 + xs[d[1]]
-
     greeted = [d for d in FAR if 0 in d]
     for d in greeted:
         pl.semaphore_signal(bar, inc=1, device_id=(peer(d), c), device_id_type=MESH)
@@ -186,11 +180,44 @@
 
     pending.append(lambda: lax.fori_loop(0, 15, a_sent, 0))
 
+    wcols = (pl.ds(0, HALF), pl.ds(HALF, HALF))
+
+    def w_one(k, d, part=None):
+        rows = slice(None) if part is None else pl.ds(16 * part, 16)
+        at = (zs[d], y) if k == 0 else (z, ys[d])
+        return WM.at[at[0], at[1], rows, wcols[k]]
+
+    def w_line(k, d, part=None):
+        group = slice(None) if part is None else pl.ds(2 * part, 2)
+        if k == 0:
+            return WM.at[group, ys[d], :, wcols[k]]
+        return WM.at[zs[d], group, :, wcols[k]]
+
+    def w_send(view, axis, k, d, step, n):
+        dev = (peer((d, 0, 0) if axis == 0 else (0, d, 0)), c)
+        n = SEM_W + n * 2 + k
+        send(view(k, *step), view(k, *step), n, n, dev).start()
+        pending.append(lambda: sent(view(k, *step), n))
+
+    def w_start(view, flip, n):
+        for k in range(2):
+            w_send(view, k ^ flip, k, 1, (0,), n)
+            w_send(view, k ^ flip, k, 3, (0,), n + 1)
+
+    def w_relay(view, flip, n):
+        for k in range(2):
+            got(view(k, 3), SEM_W + n * 2 + k)
+            w_send(view, k ^ flip, k, 1, (3, 0), n + 2)
+            got(view(k, 1), SEM_W + (n + 1) * 2 + k)
+            w_send(view, k ^ flip, k, 3, (1, 1), n + 3)
+
+    def w_end(view, n):
+        for k in range(2):
+            got(view(k, 2, 0), SEM_W + (n + 2) * 2 + k)
+            got(view(k, 2, 1), SEM_W + (n + 3) * 2 + k)
+
     wcopy.wait()
-    for d in range(1, 4):
-        dev = (ep_of((z + d) % 4, y, x), c)
-        send(WM.at[z], WM.at[z], SEM_W + d - 1, SEM_W + d - 1, dev).start()
-        pending.append(lambda d=d: sent(WM.at[z], SEM_W + d - 1))
+    w_start(w_one, 0, 0)
 
     for n in ("wi", "wo", "wst", "sb", "dr", "eld", "it", "ot", "pi", "po"):
         loads[n].wait()
@@ -252,6 +279,7 @@
             line_send(i, own[i], h, d, k)
     for i in range(3):
         hand_over(i, 0)
+    w_relay(w_one, 0, 0)
 
     loads["st"].wait()
     row = lax.broadcasted_iota(jnp.int32, (8, 512), 0)
@@ -348,6 +376,8 @@
         return 0
 
     pending.append(lambda: lax.fori_loop(0, 63, p_sent, 0))
+    w_end(w_one, 0)
+    w_start(w_line, 1, 4)
     R1[e] = SP[e]
 
     loads["routes"].wait()
@@ -411,17 +441,12 @@
         m = mixed[:, g * 512 : (g + 1) * 512]
         normed_groups.append(m * lax.rsqrt(jnp.mean(m * m, axis=1, keepdims=True) + EPSILON))
     mixer_rows = jnp.concatenate(normed_groups, axis=1) * v["gg"][...]
-    M[y, x] = mixer_rows.astype(BF)
-
-    for d in FAR_PLANE:
-        q = plane_peer(d)
-        send(M.at[y, x], M.at[y, x], SEM_M + q, SEM_M + p_own, (z * 16 + q, c)).start()
-
-    def m_sent(k, _):
-        sent(M.at[y, x], SEM_M + lax.rem(p_own + 1 + k, 16))
-        return 0
-
-    pending.append(lambda: lax.fori_loop(0, 15, m_sent, 0))
+    M[x] = mixer_rows.astype(BF)
+
+    for d in (2, 1, 3):
+        send(M.at[x], M.at[x], SEM_M + xs[d], SEM_M + x, (peer((0, 0, d)), c)).start()
+        pending.append(lambda d=d: sent(M.at[x], SEM_M + xs[d]))
+    w_relay(w_line, 1, 4)
     for new, old, fresh in ((nv_o, "pv", value_rows), (ni_o, "pi", in_rows), (no_o, "po", out_rows)):
         new[0] = v[old][1]
         new[1] = v[old][2]
@@ -449,53 +474,38 @@
 
     lax.fori_loop(0, 8, st_step, 0)
     finish()
-    for d in range(1, 4):
-        got(WM.at[(z + 4 - d) % 4], SEM_W + d - 1)
-
-    def m_got(k, _):
-        q = lax.rem(p_own + 1 + k, 16)
-        got(M.at[q // 4, q % 4], SEM_M + q)
-        return 0
-
-    lax.fori_loop(0, 15, m_got, 0)
-    part = dot(M[...].reshape(128, 2048), WM[...].reshape(128, 2048), NT)
-    SQ[...] = part.reshape(16, 8, 128).astype(BF)
-    mine = c * 16 + p_own
-
-    for d in FAR_PLANE:
-        q = plane_peer(d)
-        send(SQ.at[q], R2.at[mine], SEM_Q + q * 2 + oc, SEM_Q + mine, (z * 16 + q, oc)).start()
-        send(SQ.at[q], R2.at[mine], SEM_Q + q * 2 + c, SEM_Q + mine, (z * 16 + q, c)).start()
-    send(SQ.at[p_own], R2.at[mine], SEM_Q + p_own * 2 + oc, SEM_Q + mine, (e, oc)).start()
-
-    def q_sent(k, _):
-        q = lax.rem(p_own + 1 + k, 16)
-        sent(SQ.at[q], SEM_Q + q * 2)
-        sent(SQ.at[q], SEM_Q + q * 2 + 1)
-        return 0
-
-    pending.append(lambda: lax.fori_loop(0, 15, q_sent, 0))
-    pending.append(lambda: sent(SQ.at[p_own], SEM_Q + p_own * 2 + oc))
-    R2[mine] = SQ[p_own]
-
-    def q_got(k, _):
-        q = lax.rem(p_own + 1 + k, 16)
-        got(R2.at[q], SEM_Q + q)
-        got(R2.at[16 + q], SEM_Q + 16 + q)
-        return 0
-
-    got(R2.at[oc * 16 + p_own], SEM_Q + oc * 16 + p_own)
-    lax.fori_loop(0, 15, q_got, 0)
+    for d in (1, 3, 2):
+        got(M.at[xs[d]], SEM_M + xs[d])
+    w_end(w_line, 4)
+    part = dot(M[...].reshape(32, 2048), WM[...].reshape(512, 2048), NT)
+    SQ[...] = part.reshape(4, 8, 512).astype(BF)
+    mine = c * 4 + x
+    for d in (2, 1, 3, 0):
+        q = xs[d]
+        for other in (oc, c):
+            if d == 0 and other is c:
+                continue
+            k = SEM_Q + q * 2 + other
+            send(SQ.at[q], R2.at[mine], k, SEM_Q + mine, (peer((0, 0, d)), other)).start()
+            pending.append(lambda q=q, k=k: sent(SQ.at[q], k))
+    R2[mine] = SQ[x]
+    for d in (0, 1, 3, 2):
+        for other in (oc, c):
+            if d == 0 and other is c:
+                continue
+            k = other * 4 + xs[d]
+            got(R2.at[k], SEM_Q + k)
     tiles = [None] * 16
-    for yy in range(4):
-        a = [
-            (R2[yy * 4 + xx].astype(F32) + R2[16 + yy * 4 + xx].astype(F32)).astype(BF).astype(F32)
-            for xx in range(4)
-        ]
-        for zz in range(4):
+    a = [
+        (R2[xx].astype(F32) + R2[4 + xx].astype(F32)).astype(BF).astype(F32) for xx in range(4)
+    ]
+    for zz in range(4):
+        for yy in range(4):
             moved = [
-                a[xx] if xx == zz else pltpu.roll(a[xx], (32 * (xx - zz)) % 128, 1)
-                for xx in range(4)
+                b[:, zz * 128 : (zz + 1) * 128]
+                if xx == yy
+                else pltpu.roll(b[:, zz * 128 : (zz + 1) * 128], (32 * (xx - yy)) % 128, 1)
+                for xx, b in enumerate(a)
             ]
             tiles[zz * 4 + yy] = lane_groups(moved, lane8)
     mixed_out = jnp.concatenate(tiles, axis=1)
@@ -531,12 +541,18 @@
     for n in ("rg", "ru", "rd"):
         loads[n].wait()
 
-    for d in FAR[::-1]:
-        q = peer(d)
-        got(RX.at[c, q], SEM_X + q)
-    send(RX.at[c], RX.at[c], SEM_FX, SEM_FX, (e, oc)).start()
-    pending.append(lambda: sent(RX.at[c], SEM_FX))
-    got(RX.at[oc], SEM_FX)
+    def x_plane(h, dz):
+        return RX.at[h, pl.ds(pl.multiple_of(zs[dz] * 16, 16), 16)]
+
+    for dz in (0, 1, 3, 2):
+        for d in FAR[::-1]:
+            if d[0] == dz:
+                q = peer(d)
+                got(RX.at[c, q], SEM_X + q)
+        send(x_plane(c, dz), x_plane(c, dz), SEM_FX + dz, SEM_FX + dz, (e, oc)).start()
+        pending.append(lambda dz=dz: sent(x_plane(c, dz), SEM_FX + dz))
+    for dz in (0, 1, 3, 2):
+        got(x_plane(oc, dz), SEM_FX + dz)
     lhs = []
     for h in range(2):
         XF[...] = RX[h].astype(F32).reshape(1024, 128)
@@ -678,12 +694,12 @@
     scratch = [vm(vals[n].shape, vals[n].dtype) for n in LOADED] + [
         vm((2, 4, 4, 4, 8, HALF), BF),
         vm((4, 32, 2048), BF),
-        vm((4, 32, 2048), BF),
+        vm((4, 4, 32, 2048), BF),
         vm((64, 8, 128), BF),
         vm((64, 8, 128), BF),
-        vm((4, 4, 8, 2048), BF),
-        vm((16, 8, 128), BF),
-        vm((32, 8, 128), BF),
+        vm((4, 8, 2048), BF),
+        vm((4, 8, 512), BF),
+        vm((8, 8, 512), BF),
         vm((64, 16, 128), BF),
         vm((2, 64, 16, 128), BF),
         vm((1024, 128), F32),

time: 74.5 us -> 72.7 us (0.976)
  Pallas kernels: 73.7 us -> 71.9 us
    pallas_call x1, Pallas kernels: 70.3 us -> 68.5 us  [shards(): pl.pallas_call(layer_kernel, out_shape=[pltpu.VMEM(a, t) for a, t in shap...]
where the time goes in v3:
time: 72.7 us; the launch traced here: 72.6 us
  Pallas kernels  71.9 us (99%)
    pallas_call x1, Pallas kernels, shards(): pl.pallas_call(layer_kernel, out_shape=[pltpu.VMEM(a, t) for a, t in shap...  68.5 us
    pallas_call x1, Pallas kernels, shards(): pl.pallas_call(store_kernel, out_shape=[jax.ShapeDtypeStruct(a, t) for a,...  3.42 us

profile of v3, /device:TPU:1, one launch (start us, length us, event | category | flops | bytes accessed | tf_op | source)
XLA Modules:
  0.0 72.6 jit_solution(13505379777587082161)
XLA Ops:
  0.6 68.5 %shard_map.308 = (bf16[8,2048]{1,0:T(8,128)(2,1)S(1)}, f32[8,2048,128]{2,1,0:T(8,128)S(1)}, bf16[3,8,2048]{2,1,0:T(8,128)(2,1)S(1)}, bf16[3,8,512]{2,1,0:T(8,128)(2,1)S(1)}, bf16[3,8,512]{2,1,0:T(8,128)(2,1)S(1)}) custom-call(bf16[8,2048]{1,0:T(8,128)(2,1)} %refs_0_.1, f32[1,2048]{1,0:T(1,128)} %bitcast.36, bf16[2048,512]{1,0:T(8,128)(2,1)} %refs_2_.1, ...), custom_call_target="tpu_custom_call" | custom-call | tf_op jit(solution)/shard_map/pallas_call | solution.py:733
  69.2 3.4 %shard_map.309 = (bf16[8,2048]{1,0:T(8,128)(2,1)}, f32[8,2048,128]{2,1,0:T(8,128)}, bf16[3,8,2048]{2,1,0:T(8,128)(2,1)}, bf16[3,8,512]{2,1,0:T(8,128)(2,1)}, bf16[3,8,512]{2,1,0:T(8,128)(2,1)}) custom-call(bf16[8,2048]{1,0:T(8,128)(2,1)S(1)} %get-tuple-element.15.refs_0_, f32[8,2048,128]{2,1,0:T(8,128)S(1)} %get-tuple-element.16.refs_1_, ...), custom_call_target="tpu_custom_call" | custom-call | tf_op jit(solution)/shard_map/pallas_call | solution.py:743

commit v4 on v3

--- a/solution.py
+++ b/solution.py
@@ -118,6 +118,18 @@
     wcopy = pltpu.make_async_copy(hbm["wmt"], WM.at[z, y], ld.at[base + 4])
     loads["tok"].start()
     loads["g1"].start()
+    bar = pltpu.get_barrier_semaphore()
+    pl.semaphore_signal(bar, inc=1, device_id=(e, oc), device_id_type=MESH)
+
+    zs, ys, xs = ([(w + d) % 4 for d in range(4)] for w in own)
+
+    def peer(d):
+        return zs[d[0]] * 16 + ys[d[1]] * 4 + xs[d[2]]
+
+    greeted = [d for d in FAR if 0 in d]
+    for d in greeted:
+        pl.semaphore_signal(bar, inc=1, device_id=(peer(d), c), device_id_type=MESH)
+
     wcopy.start()
     loads["wst"].start()
     for n in ("wi", "wo", "sb", "dr", "eld", "vt", "it", "ot", "pv", "pi", "po", "hs", "gg", "g2", "routes", "cw"):
@@ -128,18 +140,6 @@
     for n in ("st", "cg", "cu", "cd", "rg", "ru", "rd"):
         loads[n].start()
 
-    bar = pltpu.get_barrier_semaphore()
-    pl.semaphore_signal(bar, inc=1, device_id=(e, oc), device_id_type=MESH)
-
-    zs, ys, xs = ([(w + d) % 4 for d in range(4)] for w in own)
-
-    def peer(d):
-        return zs[d[0]] * 16 + ys[d[1]] * 4 + xs[d[2]]
-
-    greeted = [d for d in FAR if 0 in d]
-    for d in greeted:
-        pl.semaphore_signal(bar, inc=1, device_id=(peer(d), c), device_id_type=MESH)
-
     loads["tok"].wait()
     loads["g1"].wait()
     tok = v["tok"][...].astype(F32)
@@ -162,15 +162,21 @@
     def own_piece(i):
         return X.at[c, z, y, x, :, cols(i)]
 
-    def a_send(k, _):
+    flat = sorted([(k // 4, k % 4) for k in range(1, 16)], key=hops, reverse=True)
+
+    def piece_peer(i, d):
+        full = [d[0], d[1]]
+        full.insert(i, 0)
+        return full, plane_index_of(i, full)
+
+    def plane_index_of(i, f):
+        a, b = [(zs, ys, xs)[k][f[k]] for k in range(3) if k != i]
+        return a * 4 + b
+
+    for d in flat:
         for i in range(3):
-            p = plane_index(i)
-            q = lax.rem(p + 1 + k, 16)
-            dev = (ep_of(*coords(i, own[i], q)), c)
-            send(own_piece(i), own_piece(i), SEM_A + i * 16 + q, SEM_A + i * 16 + p, dev).start()
-        return 0
-
-    lax.fori_loop(0, 15, a_send, 0)
+            full, q = piece_peer(i, d)
+            send(own_piece(i), own_piece(i), SEM_A + i * 16 + q, SEM_A + i * 16 + plane_index(i), (peer(full), c)).start()
 
     def a_sent(k, _):
         for i in range(3):
@@ -266,14 +272,10 @@
         send(plane(i, line), plane(i, line), k, k, (e, oc)).start()
         pending.append(lambda: sent(plane(i, line), k))
 
-    def a_got(k, _):
+    for d in flat[::-1]:
         for i in range(3):
-            q = lax.rem(plane_index(i) + 1 + k, 16)
-            zz, yy, xx = coords(i, own[i], q)
-            got(X.at[c, zz, yy, xx, :, cols(i)], SEM_A + i * 16 + q)
-        return 0
-
-    lax.fori_loop(0, 15, a_got, 0)
+            full, q = piece_peer(i, d)
+            got(X.at[c, zs[full[0]], ys[full[1]], xs[full[2]], :, cols(i)], SEM_A + i * 16 + q)
     for k, (h, d) in enumerate(((0, 1), (1, 3), (1, 1), (0, 3))):
         for i in range(3):
             line_send(i, own[i], h, d, k)
@@ -345,6 +347,8 @@
         got(plane(i, across, 0), SEM_B + i * 6 + 4)
         got(plane(i, across, 1), SEM_B + i * 6 + 5)
         hand_over(i, 2)
+    w_end(w_one, 0)
+    w_start(w_line, 1, 4)
     gcopy.wait()
     for w in vcopies:
         w.wait()
@@ -376,8 +380,6 @@
         return 0
 
     pending.append(lambda: lax.fori_loop(0, 63, p_sent, 0))
-    w_end(w_one, 0)
-    w_start(w_line, 1, 4)
     R1[e] = SP[e]
 
     loads["routes"].wait()

time: 72.7 us -> 68 us (0.935)
  Pallas kernels: 71.9 us -> 67.3 us
    pallas_call x1, Pallas kernels: 68.5 us -> 63.8 us  [shards(): pl.pallas_call(layer_kernel, out_shape=[pltpu.VMEM(a, t) for a, t in shap...]
where the time goes in v4:
time: 68 us; the launch traced here: 67.9 us
  Pallas kernels  67.3 us (99%)
    pallas_call x1, Pallas kernels, shards(): pl.pallas_call(layer_kernel, out_shape=[pltpu.VMEM(a, t) for a, t in shap...  63.8 us
    pallas_call x1, Pallas kernels, shards(): pl.pallas_call(store_kernel, out_shape=[jax.ShapeDtypeStruct(a, t) for a,...  3.42 us

profile of v4, /device:TPU:1, one launch (start us, length us, event | category | flops | bytes accessed | tf_op | source)
XLA Modules:
  0.0 67.9 jit_solution(16048428225106959735)
XLA Ops:
  0.6 63.8 %shard_map.308 = (bf16[8,2048]{1,0:T(8,128)(2,1)S(1)}, f32[8,2048,128]{2,1,0:T(8,128)S(1)}, bf16[3,8,2048]{2,1,0:T(8,128)(2,1)S(1)}, bf16[3,8,512]{2,1,0:T(8,128)(2,1)S(1)}, bf16[3,8,512]{2,1,0:T(8,128)(2,1)S(1)}) custom-call(bf16[8,2048]{1,0:T(8,128)(2,1)} %refs_0_.1, f32[1,2048]{1,0:T(1,128)} %bitcast.36, bf16[2048,512]{1,0:T(8,128)(2,1)} %refs_2_.1, ...), custom_call_target="tpu_custom_call" | custom-call | tf_op jit(solution)/shard_map/pallas_call | solution.py:735
  64.5 3.4 %shard_map.309 = (bf16[8,2048]{1,0:T(8,128)(2,1)}, f32[8,2048,128]{2,1,0:T(8,128)}, bf16[3,8,2048]{2,1,0:T(8,128)(2,1)}, bf16[3,8,512]{2,1,0:T(8,128)(2,1)}, bf16[3,8,512]{2,1,0:T(8,128)(2,1)}) custom-call(bf16[8,2048]{1,0:T(8,128)(2,1)S(1)} %get-tuple-element.15.refs_0_, f32[8,2048,128]{2,1,0:T(8,128)S(1)} %get-tuple-element.16.refs_1_, ...), custom_call_target="tpu_custom_call" | custom-call | tf_op jit(solution)/shard_map/pallas_call | solution.py:745

commit v5 on v4

--- a/solution.py
+++ b/solution.py
@@ -553,17 +553,23 @@
                 got(RX.at[c, q], SEM_X + q)
         send(x_plane(c, dz), x_plane(c, dz), SEM_FX + dz, SEM_FX + dz, (e, oc)).start()
         pending.append(lambda dz=dz: sent(x_plane(c, dz), SEM_FX + dz))
+    def rows_of(h):
+        XF[...] = RX[h].astype(F32).reshape(1024, 128)
+        return jnp.concatenate(
+            [XF[pl.ds(j, 128, stride=8), :].astype(BF) for j in range(8)], axis=1
+        )
+
+    theirs = pl.ds(pl.multiple_of(oc * HALF, HALF), HALF)
+    ours = pl.ds(pl.multiple_of(c * HALF, HALF), HALF)
+    rows = rows_of(c)
+    gate_sum = dot(rows, v["rg"][ours, :])
+    up_sum = dot(rows, v["ru"][ours, :])
     for dz in (0, 1, 3, 2):
         got(x_plane(oc, dz), SEM_FX + dz)
-    lhs = []
-    for h in range(2):
-        XF[...] = RX[h].astype(F32).reshape(1024, 128)
-        for j in range(8):
-            lhs.append(XF[pl.ds(j, 128, stride=8), :].astype(BF))
-    rows = jnp.concatenate(lhs, axis=1)
-    hid = (silu(dot(rows, v["rg"][...])) * dot(rows, v["ru"][...])).astype(BF)
-    theirs = pl.ds(pl.multiple_of(oc * HALF, HALF), HALF)
-    ours = pl.ds(pl.multiple_of(c * HALF, HALF), HALF)
+    rows = rows_of(oc)
+    gate_sum = gate_sum + dot(rows, v["rg"][theirs, :])
+    up_sum = up_sum + dot(rows, v["ru"][theirs, :])
+    hid = (silu(gate_sum) * up_sum).astype(BF)
     YS[...] = dot(hid, v["rd"][:, theirs]).astype(BF)
     send(YS, YR, SEM_YE, SEM_YE, (e, oc)).start()
     pending.append(lambda: sent(YS, SEM_YE))
@@ -591,10 +597,15 @@
 
     while len(pending) > 1:
         pending.pop(0)()
-    for d in FAR[::-1]:
-        q = peer(d)
-        got(RY.at[q], SEM_Y + q)
-    both = dot(CM[...], RY[...].reshape(1024, 128))
+    both = jnp.zeros((128, 128), F32)
+    for dz in (0, 1, 3, 2):
+        for d in FAR[::-1]:
+            if d[0] == dz:
+                q = peer(d)
+                got(RY.at[q], SEM_Y + q)
+        lanes = pl.ds(pl.multiple_of(zs[dz] * 256, 256), 256)
+        block = RY[pl.ds(pl.multiple_of(zs[dz] * 16, 16), 16)].reshape(256, 128)
+        both = both + dot(CM[:, lanes], block)
     comb = both[0:64] + both[64:128]
     routed = jnp.concatenate([comb[j * 8 : (j + 1) * 8] for j in range(8)], axis=1)
     res = (resid_half + routed).astype(BF)

time: 68 us -> 68.2 us (level)
  no operation moved by 1% of the time
where the time goes in v5:
time: 68.2 us; the launch traced here: 68.1 us
  Pallas kernels  67.4 us (99%)
    pallas_call x1, Pallas kernels, shards(): pl.pallas_call(layer_kernel, out_shape=[pltpu.VMEM(a, t) for a, t in shap...  64 us
    pallas_call x1, Pallas kernels, shards(): pl.pallas_call(store_kernel, out_shape=[jax.ShapeDtypeStruct(a, t) for a,...  3.42 us

profile of v5, /device:TPU:1, one launch (start us, length us, event | category | flops | bytes accessed | tf_op | source)
XLA Modules:
  0.0 68.1 jit_solution(12539203302962129088)
XLA Ops:
  0.6 64.0 %shard_map.308 = (bf16[8,2048]{1,0:T(8,128)(2,1)S(1)}, f32[8,2048,128]{2,1,0:T(8,128)S(1)}, bf16[3,8,2048]{2,1,0:T(8,128)(2,1)S(1)}, bf16[3,8,512]{2,1,0:T(8,128)(2,1)S(1)}, bf16[3,8,512]{2,1,0:T(8,128)(2,1)S(1)}) custom-call(bf16[8,2048]{1,0:T(8,128)(2,1)} %refs_0_.1, f32[1,2048]{1,0:T(1,128)} %bitcast.36, bf16[2048,512]{1,0:T(8,128)(2,1)} %refs_2_.1, ...), custom_call_target="tpu_custom_call" | custom-call | tf_op jit(solution)/shard_map/pallas_call | solution.py:746
  64.7 3.4 %shard_map.309 = (bf16[8,2048]{1,0:T(8,128)(2,1)}, f32[8,2048,128]{2,1,0:T(8,128)}, bf16[3,8,2048]{2,1,0:T(8,128)(2,1)}, bf16[3,8,512]{2,1,0:T(8,128)(2,1)}, bf16[3,8,512]{2,1,0:T(8,128)(2,1)}) custom-call(bf16[8,2048]{1,0:T(8,128)(2,1)S(1)} %get-tuple-element.15.refs_0_, f32[8,2048,128]{2,1,0:T(8,128)S(1)} %get-tuple-element.16.refs_1_, ...), custom_call_target="tpu_custom_call" | custom-call | tf_op jit(solution)/shard_map/pallas_call | solution.py:756
